TPU v7x, 32 devices: a whole 2x2x4 slice. The times are simulated.
32 devices in a mesh: sp: 16 (over z, y, core), tp: 2 (over x).
Axes of the slice: x: 2, y: 2, z: 4, core: 2. Of those that a mesh axis runs over, the one named last changes fastest.
Arguments:
- stream: bfloat16 [16384, 2048], P('sp'), may hold values from -6 to 6
- queries: bfloat16 [16384, 1024], P('sp', 'tp'), may hold values from -6 to 6
- projected_keys: bfloat16 [16384, 1024], P('sp', 'tp'), may hold values from -6 to 6
- values: bfloat16 [16384, 2048], P('sp', 'tp'), may hold values from -6 to 6
- decay_gate_logits: bfloat16 [16384, 1024], P('sp', 'tp'), may hold values from -7 to 7
- decay_gate_bias: float32 [1024], P('tp')
- extra_log_decay: float32 [16384, 8], P('sp', 'tp'), may hold values from -0.7 to 0
- document_index: int32 [16384], P('sp'), may hold values from 0 to 3, never falling along the last dimension, each value on 1 to 8192 neighbouring positions
- output_gate: bfloat16 [16384, 2048], P('sp', 'tp'), may hold values from -6 to 6
- head_norm_gain: bfloat16 [256], replicated, may hold values from 0.099609375 to 1.8984375
- output_weight: bfloat16 [2048, 2048], P('tp'), may hold values from -0.125 to 0.125
- feedforward_norm_gain: bfloat16 [2048], replicated, may hold values from 0.099609375 to 1.8984375
- gate_weight: bfloat16 [2048, 5632], P('sp', 'tp'), may hold values from -0.125 to 0.125
- up_weight: bfloat16 [2048, 5632], P('sp', 'tp'), may hold values from -0.125 to 0.125
- down_weight: bfloat16 [5632, 2048], P('tp', 'sp'), may hold values from -0.078125 to 0.078125
Outputs:
- updated: bfloat16 [16384, 2048], P(('sp', 'tp'))
All inputs are finite; a program needn't handle non-finite values.
Results may differ from a plain program's by a relative error of at most 0.015.
Values may be sent and summed in bfloat16 or wider, within the bound.
A program may use at most 128 MiB of HBM per device.

v0:
```python
import functools

import jax
import jax.numpy as jnp
from jax import lax
from jax.experimental import pallas as pl
from jax.experimental.pallas import tpu as pltpu
from jax.sharding import PartitionSpec as P

BLOCK_LENGTH = 64
TAU = 16.0
EPS = 1e-06
HIGH = lax.Precision.HIGHEST
NT = (((1,), (1,)), ((), ()))
TN = (((0,), (0,)), ((), ()))


def shard_states(blocks, size, k_ref, v_ref, decay_ref, doc_ref, cum_ref, state_ref, log_ref,
                 tail_ref, lead_ref):
    rows = lax.broadcasted_iota(jnp.int32, (size, size), 0)
    cols = lax.broadcasted_iota(jnp.int32, (size, size), 1)
    lower = (cols <= rows).astype(jnp.float32)
    before = jnp.zeros((1, k_ref.shape[1]), jnp.float32)
    starts = []
    for b in range(blocks):
        here = pl.ds(b * size, size)
        cum = jnp.dot(lower, decay_ref[here, :], precision=HIGH,
                      preferred_element_type=jnp.float32)
        cum_ref[here, :] = cum
        starts.append(before)
        before = before + cum[size - 1 : size]
    total = before
    first = doc_ref[0:1, :]
    last = doc_ref[blocks * size - 1 : blocks * size, :]
    for b in range(blocks):
        here = pl.ds(b * size, size)
        cum = cum_ref[here, :] + starts[b]
        keys = k_ref[here, :].astype(jnp.float32)
        doc = doc_ref[here, :]
        tail_ref[here, :] = jnp.where(doc == last, keys * jnp.exp(total - cum), 0.0).astype(
            jnp.bfloat16)
        lead_ref[here, :] = jnp.where(doc == first, keys * jnp.exp(cum), 0.0).astype(
            jnp.bfloat16)
    values = v_ref[...]
    state_ref[0, 0] = lax.dot_general(
        tail_ref[...], values, TN, preferred_element_type=jnp.float32).astype(jnp.bfloat16)
    state_ref[1, 0] = lax.dot_general(
        lead_ref[...], values, TN, preferred_element_type=jnp.float32).astype(jnp.bfloat16)
    log_ref[0] = jnp.broadcast_to(total, log_ref.shape[1:])


def head_outputs(blocks, size, q_ref, k_ref, v_ref, cum_ref, doc_ref, same_ref, gate_ref,
                 gain_ref, carry_ref, out_ref, back_ref):
    scale = q_ref.shape[1] ** (-0.5)
    later = carry_ref[1, 0]
    for b in reversed(range(blocks)):
        here = pl.ds(b * size, size)
        back_ref[b] = later.astype(jnp.bfloat16)
        if b:
            cum = cum_ref[here, :]
            doc = doc_ref[here, :]
            first, last = doc[0:1], doc[size - 1 : size]
            previous = doc_ref[b * size - 1 : b * size, :]
            lead = jnp.where(doc == first, k_ref[here, :].astype(jnp.float32) * jnp.exp(cum), 0.0)
            added = lax.dot_general(lead.astype(jnp.bfloat16), v_ref[here, :], TN,
                                    preferred_element_type=jnp.float32)
            through = jnp.where(first == last, jnp.exp(cum[size - 1 : size]), 0.0)
            later = added + jnp.transpose(through) * later
            later = jnp.where(jnp.transpose(previous == first), later, 0.0)
    earlier = carry_ref[0, 0]
    rows = lax.broadcasted_iota(jnp.int32, (size, size), 0)
    cols = lax.broadcasted_iota(jnp.int32, (size, size), 1)
    for b in range(blocks):
        here = pl.ds(b * size, size)
        cum = cum_ref[here, :]
        doc = doc_ref[here, :]
        first, last = doc[0:1], doc[size - 1 : size]
        end = cum[size - 1 : size]
        query = q_ref[here, :].astype(jnp.float32) * scale
        keys = k_ref[here, :].astype(jnp.float32)
        values = v_ref[here, :]
        middle = cum[size // 2 - 1 : size // 2]
        rising = jnp.exp(cum - middle)
        falling = jnp.exp(middle - cum)
        forward = lax.dot_general((query * rising).astype(jnp.bfloat16),
                                  (keys * falling).astype(jnp.bfloat16), NT,
                                  preferred_element_type=jnp.float32)
        backward = lax.dot_general((query * falling).astype(jnp.bfloat16),
                                   (keys * rising).astype(jnp.bfloat16), NT,
                                   preferred_element_type=jnp.float32)
        same = same_ref[here, :] > 0.0
        scores = jnp.where(same & (cols <= rows), forward, 0.0) + jnp.where(
            same & (cols >= rows), backward, 0.0)
        total = jnp.dot(scores.astype(jnp.bfloat16), values, preferred_element_type=jnp.float32)
        shrink = jnp.exp(end - cum)
        onward = jnp.where(doc == first, query * jnp.exp(cum), 0.0).astype(jnp.bfloat16)
        rearward = jnp.where(doc == last, query * shrink, 0.0).astype(jnp.bfloat16)
        total = total + jnp.dot(onward, earlier.astype(jnp.bfloat16),
                                preferred_element_type=jnp.float32)
        total = total + jnp.dot(rearward, back_ref[b], preferred_element_type=jnp.float32)
        if b < blocks - 1:
            tail = jnp.where(doc == last, keys * shrink, 0.0)
            added = lax.dot_general(tail.astype(jnp.bfloat16), values, TN,
                                    preferred_element_type=jnp.float32)
            through = jnp.where(first == last, jnp.exp(end), 0.0)
            following = doc_ref[(b + 1) * size : (b + 1) * size + 1, :]
            earlier = added + jnp.transpose(through) * earlier
            earlier = jnp.where(jnp.transpose(last == following), earlier, 0.0)
        scaled = total * lax.rsqrt(jnp.mean(total * total, axis=-1, keepdims=True) + EPS)
        gate = gate_ref[here, :].astype(jnp.float32)
        scaled = scaled * gain_ref[...] * (gate / (1.0 + jnp.exp(-gate)))
        out_ref[here, :] = scaled.astype(jnp.bfloat16)


def row_norm(rows_f, gain):
    factor = lax.rsqrt(jnp.mean(rows_f * rows_f, axis=-1, keepdims=True) + EPS)
    return (rows_f * factor * gain.astype(jnp.float32)).astype(jnp.bfloat16)


def product(a, b):
    return jnp.dot(a, b, preferred_element_type=jnp.float32)


def carried_in(state, logs, leaves, enters, way):
    size = lax.axis_size("sp")
    me = lax.axis_index("sp")

    def from_away(distance, state, small):
        pairs = [(s, s + way * distance) for s in range(size) if 0 <= s + way * distance < size]
        return (lax.ppermute(state, "sp", pairs), lax.ppermute(small, "sp", pairs))

    def packed(logs, document):
        return jnp.concatenate([logs, jnp.full((1, logs.shape[1]), document)])

    state, small = from_away(1, state, packed(logs, leaves))
    place = me if way > 0 else size - 1 - me
    have = place >= 1
    state = jnp.where(have, state.astype(jnp.float32), 0.0)
    logs = jnp.where(have, small[:-1], 0.0)
    document = jnp.where(have, small[-1, 0], -1.0)
    distance = 1
    while distance < size - 1:
        far, small = from_away(distance, state.astype(jnp.bfloat16), packed(logs, document))
        reach = (place > distance) & (small[-1, 0] == document)
        weight = jnp.where(reach, jnp.exp(logs), 0.0)
        state = state + weight[..., None] * far.astype(jnp.float32)
        logs = logs + small[:-1]
        distance *= 2
    return jnp.where(document == enters, state, 0.0)


def attention(queries, projected_keys, values, decay_gate_logits, decay_gate_bias,
              extra_log_decay, document_index, output_gate, head_norm_gain, up_weight, gate_full):
    heads = extra_log_decay.shape[1]
    rows = queries.shape[0]
    dk = queries.shape[1] // heads
    dv = values.shape[1] // heads
    size = BLOCK_LENGTH
    blocks = rows // size
    decay = jax.nn.log_sigmoid(decay_gate_logits.astype(jnp.float32) + decay_gate_bias) / TAU
    decay = (decay.reshape(rows, heads, dk) + extra_log_decay[:, :, None]).reshape(rows, -1)
    doc = document_index.astype(jnp.float32)
    doc_wide = jnp.broadcast_to(doc[:, None], (rows, dk))
    by_block = doc.reshape(blocks, size)
    same = (by_block[:, :, None] == by_block[:, None, :]).astype(jnp.float32).reshape(rows, size)
    keyed = pl.BlockSpec((rows, dk), lambda h: (0, h))
    valued = pl.BlockSpec((rows, dv), lambda h: (0, h))
    fixed = pl.BlockSpec((rows, dk), lambda h: (0, 0))
    state_spec = pl.BlockSpec((2, 1, dk, dv), lambda h: (0, h, 0, 0))
    params = pltpu.CompilerParams(dimension_semantics=("arbitrary",),
                                  vmem_limit_bytes=40 * 1024 * 1024)
    cum, states, logs = pl.pallas_call(
        functools.partial(shard_states, blocks, size),
        grid=(heads,),
        out_shape=(
            jax.ShapeDtypeStruct((rows, heads * dk), jnp.float32),
            jax.ShapeDtypeStruct((2, heads, dk, dv), jnp.bfloat16),
            jax.ShapeDtypeStruct((heads, 8, dk), jnp.float32),
        ),
        in_specs=[keyed, valued, keyed, fixed],
        out_specs=(keyed, state_spec, pl.BlockSpec((1, 8, dk), lambda h: (h, 0, 0))),
        scratch_shapes=[pltpu.VMEM((rows, dk), jnp.bfloat16)] * 2,
        compiler_params=params,
        cost_estimate=pl.CostEstimate(flops=rows * heads * dk * dv * 4,
                                      bytes_accessed=rows * heads * dk * 20,
                                      transcendentals=rows * heads * dk * 2),
        name="shard_states",
    )(projected_keys, values, decay, doc_wide)
    first, last = doc[0], doc[rows - 1]
    logs = logs[:, 0]
    ahead = carried_in(states[0], logs, last, first, 1)
    ahead, up_weight, gate_full = lax.optimization_barrier((ahead, up_weight, gate_full))
    carry = jnp.stack([ahead, carried_in(states[1], logs, first, last, -1)])
    mixed = pl.pallas_call(
        functools.partial(head_outputs, blocks, size),
        grid=(heads,),
        out_shape=jax.ShapeDtypeStruct((rows, heads * dv), jnp.bfloat16),
        in_specs=[keyed, keyed, valued, keyed, fixed,
                  pl.BlockSpec((rows, size), lambda h: (0, 0)), valued,
                  pl.BlockSpec((1, dv), lambda h: (0, 0)), state_spec],
        out_specs=valued,
        scratch_shapes=[pltpu.VMEM((blocks, dk, dv), jnp.bfloat16)],
        compiler_params=params,
        cost_estimate=pl.CostEstimate(flops=rows * heads * dk * dv * 10,
                                      bytes_accessed=rows * heads * dk * 24,
                                      transcendentals=rows * heads * dk * 8),
        name="head_outputs",
    )(queries, projected_keys, values, cum, doc_wide, same, output_gate,
      head_norm_gain.astype(jnp.float32)[None], carry)
    return mixed, up_weight, gate_full


def per_device(stream, queries, projected_keys, values, decay_gate_logits, decay_gate_bias,
               extra_log_decay, document_index, output_gate, head_norm_gain, output_weight,
               feedforward_norm_gain, gate_weight, up_weight, down_weight):
    tp = lax.axis_size("tp")
    gather = lambda w, axis: lax.all_gather(w, "sp", axis=axis, tiled=True)
    gate_full = gather(gate_weight, 0)
    mixed, up_weight, gate_full = attention(
        queries, projected_keys, values, decay_gate_logits, decay_gate_bias, extra_log_decay,
        document_index, output_gate, head_norm_gain, up_weight, gate_full)
    up_full = gather(up_weight, 0)

    def hidden_of(normed):
        gate = product(normed, gate_full)
        up = product(normed, up_full)
        return (jax.nn.silu(gate) * up).astype(jnp.bfloat16)

    def down_of(hidden):
        return product(hidden, down_full).astype(jnp.bfloat16)

    share = stream.shape[0] // tp
    start = lax.axis_index("tp") * share
    own_stream = lax.dynamic_slice_in_dim(stream, start, share, 0).astype(jnp.float32)
    if tp == 2:
        swap = lambda x: lax.ppermute(x, "tp", [(0, 1), (1, 0)])
        chunks = 2
        step = share // chunks
        other = share - start
        rows_of = lambda x, base, c: lax.dynamic_slice_in_dim(x, base + c * step, step, 0)
        sent = [swap(product(rows_of(mixed, other, c), output_weight).astype(jnp.bfloat16))
                for c in range(chunks)]
        sent, up_full, down_weight = lax.optimization_barrier((sent, up_full, down_weight))
        down_full = gather(down_weight, 1)
        resid, normed = [], []
        for c in range(chunks):
            kept = product(rows_of(mixed, start, c), output_weight).astype(jnp.bfloat16)
            resid.append(own_stream[c * step : (c + 1) * step]
                         + (kept.astype(jnp.float32) + sent[c].astype(jnp.float32)))
            normed.append(row_norm(resid[c], feedforward_norm_gain))
        away = [swap(n) for n in normed]
        hidden_away = [hidden_of(n) for n in away]
        hidden_own = hidden_of(jnp.concatenate(normed))
        hidden_away, hidden_own, down_full = lax.optimization_barrier(
            (hidden_away, hidden_own, down_full))
        partial = [down_of(h) for h in hidden_away]
        partial, hidden_own = lax.optimization_barrier((partial, hidden_own))
        returned = [swap(p) for p in partial]
        kept = down_of(hidden_own)
        return jnp.concatenate([
            (resid[c] + (kept[c * step : (c + 1) * step].astype(jnp.float32)
                         + returned[c].astype(jnp.float32))).astype(jnp.bfloat16)
            for c in range(chunks)])
    down_full = gather(down_weight, 1)
    scatter = lambda x: lax.psum_scatter(x, "tp", scatter_dimension=0, tiled=True)
    attended = scatter(product(mixed, output_weight).astype(jnp.bfloat16)).astype(jnp.float32)
    resid = own_stream + attended
    normed = lax.all_gather(row_norm(resid, feedforward_norm_gain), "tp", axis=0, tiled=True)
    mlp_out = scatter(down_of(hidden_of(normed))).astype(jnp.float32)
    return (resid + mlp_out).astype(jnp.bfloat16)


def solution(mesh):
    placed = (
        P("sp", None),
        P("sp", "tp"),
        P("sp", "tp"),
        P("sp", "tp"),
        P("sp", "tp"),
        P("tp"),
        P("sp", "tp"),
        P("sp"),
        P("sp", "tp"),
        P(),
        P("tp", None),
        P(),
        P("sp", "tp"),
        P("sp", "tp"),
        P("tp", "sp"),
    )
    return jax.shard_map(
        per_device, mesh=mesh, in_specs=placed, out_specs=P(("sp", "tp"), None), check_vma=False
    )
```

profile of v0, /device:TPU:0, one launch (start us, length us, event | category | flops | bytes accessed | tf_op | source)
XLA Modules:
  0.0 454.2 jit_solution(11339783105420147662)
XLA Ops:
  12.1 4.9 %shard_states.1 = (f32[1024,512]{1,0:T(8,128)S(1)}, bf16[2,4,128,256]{3,2,1,0:T(8,128)(2,1)S(1)}, f32[4,8,128]{2,1,0:T(8,128)S(1)}) custom-call(bf16[1024,512]{1,0:T(8,128)(2,1)S(1)} %copy-done.1, bf16[1024,1024]{1,0:T(8,128)(2,1)S(1)} %copy-done, f32[1024,512]{1,0:T(8,128)S(1)} %fusion.4.decay_ref, f32[1024,128]{1,0:T(8,128)S(1)} %broadcast_in_dim.26.doc_ref), custom_call_target="tpu_custom_call" | custom-call | flops 536870912 | bytes 10485760 | tf_op jit(solution)/shard_map/shard_states/pallas_call | solution.py:172
  23.4 4.5 collective-permute-start
  28.0 5.7 %collective-permute-start.3 = (bf16[4,128,256]{2,1,0:T(8,128)(2,1)S(1)}, bf16[4,128,256]{2,1,0:T(8,128)(2,1)S(1)}, u32[]{:S(2)}, u32[]{:S(2)}) collective-permute-start(bf16[4,128,256]{2,1,0:T(8,128)(2,1)S(1)} %fusion.11), channel_id=1, source_target_pairs={{0,2},{2,4},{4,6},{6,8},{8,10},{10,12},{12,14},{14,16},{16,18},{18... | collective-permute-start | bytes 786440 | tf_op jit(solution)/shard_map/ppermute | solution.py:130
  34.8 4.4 collective-permute-start.2
  41.9 5.8 %collective-permute-start.5 = (bf16[4,128,256]{2,1,0:T(8,128)(2,1)}, bf16[4,128,256]{2,1,0:T(8,128)(2,1)S(1)}, u32[]{:S(2)}, u32[]{:S(2)}) collective-permute-start(bf16[4,128,256]{2,1,0:T(8,128)(2,1)} %fusion.13), channel_id=1, source_target_pairs={{0,4},{2,6},{4,8},{6,10},{8,12},{10,14},{12,16},{14,18},{16,20},{1... | collective-permute-start | bytes 786440 | tf_op jit(solution)/shard_map/ppermute | solution.py:130
  47.7 10.5 %collective-permute-start.4 = (f32[5,128]{1,0:T(8,128)S(1)}, f32[5,128]{1,0:T(8,128)S(1)}, u32[]{:S(2)}, u32[]{:S(2)}) collective-permute-start(f32[5,128]{1,0:T(8,128)S(1)} %concatenate.38), channel_id=1, source_target_pairs={{0,4},{2,6},{4,8},{6,10},{8,12},{10,14},{12,16},{14,18},{16,20},{1... | collective-permute-start | bytes 7688 | tf_op jit(solution)/shard_map/ppermute | solution.py:130
  61.6 9.9 %collective-permute-start.7 = (bf16[4,128,256]{2,1,0:T(8,128)(2,1)}, bf16[4,128,256]{2,1,0:T(8,128)(2,1)}, u32[]{:S(2)}, u32[]{:S(2)}) collective-permute-start(bf16[4,128,256]{2,1,0:T(8,128)(2,1)} %fusion.27), channel_id=1, source_target_pairs={{0,8},{2,10},{4,12},{6,14},{8,16},{10,18},{12,20},{14,22},{16,24},... | collective-permute-start | bytes 786440 | tf_op jit(solution)/shard_map/ppermute | solution.py:130
  71.4 14.6 %collective-permute-start.6 = (f32[5,128]{1,0:T(8,128)S(1)}, f32[5,128]{1,0:T(8,128)S(1)}, u32[]{:S(2)}, u32[]{:S(2)}) collective-permute-start(f32[5,128]{1,0:T(8,128)S(1)} %concatenate.39), channel_id=1, source_target_pairs={{0,8},{2,10},{4,12},{6,14},{8,16},{10,18},{12,20},{14,22},{16,24},... | collective-permute-start | bytes 7688 | tf_op jit(solution)/shard_map/ppermute | solution.py:130
  90.4 15.3 %collective-permute-start.9 = (bf16[4,128,256]{2,1,0:T(8,128)(2,1)}, bf16[4,128,256]{2,1,0:T(8,128)(2,1)}, u32[]{:S(2)}, u32[]{:S(2)}) collective-permute-start(bf16[4,128,256]{2,1,0:T(8,128)(2,1)} %fusion.15), channel_id=1, source_target_pairs={{0,16},{2,18},{4,20},{6,22},{8,24},{10,26},{12,28},{14,30},{1,17},... | collective-permute-start | bytes 786440 | tf_op jit(solution)/shard_map/ppermute | solution.py:130
  107.7 6.9 %collective-permute-done.8 = f32[5,128]{1,0:T(8,128)S(1)} collective-permute-done((f32[5,128]{1,0:T(8,128)S(1)}, f32[5,128]{1,0:T(8,128)S(1)}, u32[]{:S(2)}, u32[]{:S(2)}) %collective-permute-start.8) | collective-permute-done | bytes 2592 | tf_op jit(solution)/shard_map/ppermute | solution.py:130
  125.5 8.4 %collective-permute-done.12 = f32[5,128]{1,0:T(8,128)S(1)} collective-permute-done((f32[5,128]{1,0:T(8,128)S(1)}, f32[5,128]{1,0:T(8,128)S(1)}, u32[]{:S(2)}, u32[]{:S(2)}) %collective-permute-start.12) | collective-permute-done | bytes 2592 | tf_op jit(solution)/shard_map/ppermute | solution.py:130
  138.4 15.6 %collective-permute-done.14 = f32[5,128]{1,0:T(8,128)S(1)} collective-permute-done((f32[5,128]{1,0:T(8,128)S(1)}, f32[5,128]{1,0:T(8,128)S(1)}, u32[]{:S(2)}, u32[]{:S(2)}) %collective-permute-start.14) | collective-permute-done | bytes 2592 | tf_op jit(solution)/shard_map/ppermute | solution.py:130
  158.8 17.3 %collective-permute-done.16 = f32[5,128]{1,0:T(8,128)S(1)} collective-permute-done((f32[5,128]{1,0:T(8,128)S(1)}, f32[5,128]{1,0:T(8,128)S(1)}, u32[]{:S(2)}, u32[]{:S(2)}) %collective-permute-start.16) | collective-permute-done | bytes 2592 | tf_op jit(solution)/shard_map/ppermute | solution.py:130
  183.3 29.8 %collective-permute-done.18 = f32[5,128]{1,0:T(8,128)S(1)} collective-permute-done((f32[5,128]{1,0:T(8,128)S(1)}, f32[5,128]{1,0:T(8,128)S(1)}, u32[]{:S(2)}, u32[]{:S(2)}) %collective-permute-start.18) | collective-permute-done | bytes 2592 | tf_op jit(solution)/shard_map/ppermute | solution.py:130
  220.0 17.8 %head_outputs.1 = bf16[1024,1024]{1,0:T(8,128)(2,1)S(1)} custom-call(bf16[1024,512]{1,0:T(8,128)(2,1)S(1)} %copy-done.8, bf16[1024,512]{1,0:T(8,128)(2,1)S(1)} %copy-done.2, bf16[1024,1024]{1,0:T(8,128)(2,1)S(1)} %copy-done, f32[1024,512]{1,0:T(8,128)S(1)} %copy-done.5, f32[1024,128]{1,0:T(8,128)S(1)} %broadcast_in_dim.26.doc_ref, ...), custom_call_target="tpu_custom_call" | custom-call | flops 1342177280 | bytes 12582912 | tf_op jit(solution)/shard_map/head_outputs/pallas_call | solution.py:194
  242.5 22.7 %collective-permute-done.21 = bf16[256,2048]{1,0:T(8,128)(2,1)S(1)} collective-permute-done((bf16[256,2048]{1,0:T(8,128)(2,1)S(1)}, bf16[256,2048]{1,0:T(8,128)(2,1)S(1)}, u32[]{:S(2)}, u32[]{:S(2)}) %collective-permute-start.21) | collective-permute-done | bytes 1048608 | tf_op jit(solution)/shard_map/ppermute | solution.py:236
  265.2 21.7 %collective-permute-done.20 = bf16[256,2048]{1,0:T(8,128)(2,1)S(1)} collective-permute-done((bf16[256,2048]{1,0:T(8,128)(2,1)S(1)}, bf16[256,2048]{1,0:T(8,128)(2,1)S(1)}, u32[]{:S(2)}, u32[]{:S(2)}) %collective-permute-start.20) | collective-permute-done | bytes 1048608 | tf_op jit(solution)/shard_map/ppermute | solution.py:236
  291.3 2.9 multiply_reduce_fusion.1
  299.2 6.1 %fusion.5 = f32[512,2816]{1,0:T(8,128)S(1)} fusion(bf16[2048,2816]{1,0:T(8,128)(2,1)S(1)} %bitcast.53, bf16[256,2048]{1,0:T(8,128)(2,1)S(1)} %get-tuple-element.43, bf16[256,2048]{1,0:T(8,128)(2,1)S(1)} %get-tuple-element.44), kind=kOutput, calls=%fused_computation.27 | convolution fusion | flops 5909774336 | bytes 19398656 | tf_op jit(solution)/shard_map/dot_general | solution.py:121
  305.3 12.8 %multiply_convert_fusion = bf16[512,2816]{1,0:T(8,128)(2,1)} fusion(f32[512,2816]{1,0:T(8,128)S(1)} %fusion.5, bf16[2048,2816]{1,0:T(8,128)(2,1)} %all-gather.6.cloned.1.call-done, bf16[256,2048]{1,0:T(8,128)(2,1)S(1)} %get-tuple-element.43, bf16[256,2048]{1,0:T(8,128)(2,1)S(1)} %get-tuple-element.44), kind=kOutput, calls=%fused_computation.1 | convolution fusion | flops 5918425088 | bytes 22282240 | tf_op jit(solution)/shard_map/dot_general | solution.py:121
  318.1 5.1 %collective-permute-done.23 = bf16[256,2048]{1,0:T(8,128)(2,1)S(1)} collective-permute-done((bf16[256,2048]{1,0:T(8,128)(2,1)S(1)}, bf16[256,2048]{1,0:T(8,128)(2,1)S(1)}, u32[]{:S(2)}, u32[]{:S(2)}) %collective-permute-start.23) | collective-permute-done | bytes 1048608 | tf_op jit(solution)/shard_map/ppermute | solution.py:236
  323.2 3.1 fusion.32
  326.3 17.7 %collective-permute-done.22 = bf16[256,2048]{1,0:T(8,128)(2,1)S(1)} collective-permute-done((bf16[256,2048]{1,0:T(8,128)(2,1)S(1)}, bf16[256,2048]{1,0:T(8,128)(2,1)S(1)}, u32[]{:S(2)}, u32[]{:S(2)}) %collective-permute-start.22) | collective-permute-done | bytes 1048608 | tf_op jit(solution)/shard_map/ppermute | solution.py:236
  344.1 3.1 fusion.31
  347.2 9.5 %multiply_convert_fusion.1 = bf16[256,2816]{1,0:T(8,128)(2,1)} fusion(f32[256,2816]{1,0:T(8,128)S(1)} %fusion.32, bf16[256,2048]{1,0:T(8,128)(2,1)S(1)} %collective-permute-done.23, bf16[2048,2816]{1,0:T(8,128)(2,1)} %all-gather.6.cloned.1.call-done), kind=kOutput, calls=%fused_computation.3 | convolution fusion | flops 2957115392 | bytes 16908288 | tf_op jit(solution)/shard_map/dot_general | solution.py:121
  356.7 5.5 %multiply_convert_fusion.2 = bf16[256,2816]{1,0:T(8,128)(2,1)} fusion(f32[256,2816]{1,0:T(8,128)S(1)} %fusion.31, bf16[256,2048]{1,0:T(8,128)(2,1)S(1)} %collective-permute-done.22, bf16[2048,2816]{1,0:T(8,128)(2,1)S(1)} %bitcast.55), kind=kOutput, calls=%fused_computation.4 | convolution fusion | flops 2957115392 | bytes 16908288 | tf_op jit(solution)/shard_map/dot_general | solution.py:121
  362.3 23.1 %all-gather.8.cloned.1.call-done = bf16[2816,2048]{1,0:T(8,128)(2,1)} async-done(((bf16[2816,128]{1,0:T(8,128)(2,1)}), bf16[2816,2048]{1,0:T(8,128)(2,1)}) %all-gather.8.cloned.1.call-update) | async-done | bytes 11534352 | tf_op jit(solution)/shard_map/all_gather | solution.py:217
  385.3 8.0 %convolution_convert_fusion.1 = bf16[256,2048]{1,0:T(8,128)(2,1)S(1)} fusion(bf16[256,2816]{1,0:T(8,128)(2,1)} %multiply_convert_fusion.1, bf16[2816,2048]{1,0:T(8,128)(2,1)} %all-gather.8.cloned.1.call-done), kind=kOutput, calls=%fused_computation.5 | convolution fusion | flops 2953314304 | bytes 14024704 | tf_op jit(solution)/shard_map/dot_general | solution.py:121
  393.7 3.2 convolution_convert_fusion.2
  399.0 6.3 %convolution_convert_fusion = bf16[512,2048]{1,0:T(8,128)(2,1)S(1)} fusion(bf16[512,2816]{1,0:T(8,128)(2,1)S(1)} %copy-done.26, bf16[2816,2048]{1,0:T(8,128)(2,1)S(1)} %copy-done.16), kind=kOutput, calls=%fused_computation.2 | convolution fusion | flops 5906628608 | bytes 16515072 | tf_op jit(solution)/shard_map/dot_general | solution.py:121
  405.3 17.7 %collective-permute-done.24 = bf16[256,2048]{1,0:T(8,128)(2,1)S(1)} collective-permute-done((bf16[256,2048]{1,0:T(8,128)(2,1)S(1)}, bf16[256,2048]{1,0:T(8,128)(2,1)S(1)}, u32[]{:S(2)}, u32[]{:S(2)}) %collective-permute-start.24) | collective-permute-done | bytes 1048608 | tf_op jit(solution)/shard_map/ppermute | solution.py:236
  423.0 21.8 %collective-permute-done.25 = bf16[256,2048]{1,0:T(8,128)(2,1)S(1)} collective-permute-done((bf16[256,2048]{1,0:T(8,128)(2,1)S(1)}, bf16[256,2048]{1,0:T(8,128)(2,1)S(1)}, u32[]{:S(2)}, u32[]{:S(2)}) %collective-permute-start.25) | collective-permute-done | bytes 1048608 | tf_op jit(solution)/shard_map/ppermute | solution.py:236
  (169 shorter events, 70.9 us)
Async XLA Ops:
  6.5 111.5 %all-gather.4.cloned.1.call-start = ((), (), s32[]{:S(2)}) async-start(), calls=%async_computation | async-start | bytes 12255232 | tf_op jit(solution)/shard_map/all_gather | solution.py:217
  7.3 279.6 %all-gather.6.cloned.1.call-start = ((), (), s32[]{:S(2)}) async-start(), calls=%async_computation.1 | async-start | bytes 12255232 | tf_op jit(solution)/shard_map/all_gather | solution.py:217
  19.1 8.9 %collective-permute-start.1 = (bf16[4,128,256]{2,1,0:T(8,128)(2,1)S(1)}, bf16[4,128,256]{2,1,0:T(8,128)(2,1)S(1)}, u32[]{:S(2)}, u32[]{:S(2)}) collective-permute-start(bf16[4,128,256]{2,1,0:T(8,128)(2,1)S(1)} %get-tuple-element.41), channel_id=1, source_target_pairs={{0,2},{2,4},{4,6},{6,8},{8,10},{10,12},{12,14},{14,16},{16,18},{18... | collective-permute-start | bytes 786440 | tf_op jit(solution)/shard_map/ppermute | solution.py:130
  23.4 10.3 %collective-permute-start = (f32[5,128]{1,0:T(8,128)S(1)}, f32[5,128]{1,0:T(8,128)S(1)}, u32[]{:S(2)}, u32[]{:S(2)}) collective-permute-start(f32[5,128]{1,0:T(8,128)S(1)} %get-tuple-element.53), channel_id=1, source_target_pairs={{0,2},{2,4},{4,6},{6,8},{8,10},{10,12},{12,14},{14,16},{16,18},{18... | collective-permute-start | bytes 7688 | tf_op jit(solution)/shard_map/ppermute | solution.py:130
  28.0 13.0 %collective-permute-start.3 = (bf16[4,128,256]{2,1,0:T(8,128)(2,1)S(1)}, bf16[4,128,256]{2,1,0:T(8,128)(2,1)S(1)}, u32[]{:S(2)}, u32[]{:S(2)}) collective-permute-start(bf16[4,128,256]{2,1,0:T(8,128)(2,1)S(1)} %fusion.11), channel_id=1, source_target_pairs={{0,2},{2,4},{4,6},{6,8},{8,10},{10,12},{12,14},{14,16},{16,18},{18... | collective-permute-start | bytes 786440 | tf_op jit(solution)/shard_map/ppermute | solution.py:130
  34.8 5.2 %collective-permute-start.2 = (f32[5,128]{1,0:T(8,128)S(1)}, f32[5,128]{1,0:T(8,128)S(1)}, u32[]{:S(2)}, u32[]{:S(2)}) collective-permute-start(f32[5,128]{1,0:T(8,128)S(1)} %concatenate.37), channel_id=1, source_target_pairs={{0,2},{2,4},{4,6},{6,8},{8,10},{10,12},{12,14},{14,16},{16,18},{18... | collective-permute-start | bytes 7688 | tf_op jit(solution)/shard_map/ppermute | solution.py:130
  41.9 18.7 %collective-permute-start.5 = (bf16[4,128,256]{2,1,0:T(8,128)(2,1)}, bf16[4,128,256]{2,1,0:T(8,128)(2,1)S(1)}, u32[]{:S(2)}, u32[]{:S(2)}) collective-permute-start(bf16[4,128,256]{2,1,0:T(8,128)(2,1)} %fusion.13), channel_id=1, source_target_pairs={{0,4},{2,6},{4,8},{6,10},{8,12},{10,14},{12,16},{14,18},{16,20},{1... | collective-permute-start | bytes 786440 | tf_op jit(solution)/shard_map/ppermute | solution.py:130
  47.7 11.9 %collective-permute-start.4 = (f32[5,128]{1,0:T(8,128)S(1)}, f32[5,128]{1,0:T(8,128)S(1)}, u32[]{:S(2)}, u32[]{:S(2)}) collective-permute-start(f32[5,128]{1,0:T(8,128)S(1)} %concatenate.38), channel_id=1, source_target_pairs={{0,4},{2,6},{4,8},{6,10},{8,12},{10,14},{12,16},{14,18},{16,20},{1... | collective-permute-start | bytes 7688 | tf_op jit(solution)/shard_map/ppermute | solution.py:130
  61.6 26.9 %collective-permute-start.7 = (bf16[4,128,256]{2,1,0:T(8,128)(2,1)}, bf16[4,128,256]{2,1,0:T(8,128)(2,1)}, u32[]{:S(2)}, u32[]{:S(2)}) collective-permute-start(bf16[4,128,256]{2,1,0:T(8,128)(2,1)} %fusion.27), channel_id=1, source_target_pairs={{0,8},{2,10},{4,12},{6,14},{8,16},{10,18},{12,20},{14,22},{16,24},... | collective-permute-start | bytes 786440 | tf_op jit(solution)/shard_map/ppermute | solution.py:130
  71.4 16.0 %collective-permute-start.6 = (f32[5,128]{1,0:T(8,128)S(1)}, f32[5,128]{1,0:T(8,128)S(1)}, u32[]{:S(2)}, u32[]{:S(2)}) collective-permute-start(f32[5,128]{1,0:T(8,128)S(1)} %concatenate.39), channel_id=1, source_target_pairs={{0,8},{2,10},{4,12},{6,14},{8,16},{10,18},{12,20},{14,22},{16,24},... | collective-permute-start | bytes 7688 | tf_op jit(solution)/shard_map/ppermute | solution.py:130
  90.4 25.4 %collective-permute-start.9 = (bf16[4,128,256]{2,1,0:T(8,128)(2,1)}, bf16[4,128,256]{2,1,0:T(8,128)(2,1)}, u32[]{:S(2)}, u32[]{:S(2)}) collective-permute-start(bf16[4,128,256]{2,1,0:T(8,128)(2,1)} %fusion.15), channel_id=1, source_target_pairs={{0,16},{2,18},{4,20},{6,22},{8,24},{10,26},{12,28},{14,30},{1,17},... | collective-permute-start | bytes 786440 | tf_op jit(solution)/shard_map/ppermute | solution.py:130
  105.7 8.8 %collective-permute-start.8 = (f32[5,128]{1,0:T(8,128)S(1)}, f32[5,128]{1,0:T(8,128)S(1)}, u32[]{:S(2)}, u32[]{:S(2)}) collective-permute-start(f32[5,128]{1,0:T(8,128)S(1)} %concatenate.40), channel_id=1, source_target_pairs={{0,16},{2,18},{4,20},{6,22},{8,24},{10,26},{12,28},{14,30},{1,17},... | collective-permute-start | bytes 7688 | tf_op jit(solution)/shard_map/ppermute | solution.py:130
  118.1 267.2 %all-gather.8.cloned.1.call-start = ((), (), s32[]{:S(2)}) async-start(), calls=%async_computation.2 | async-start | bytes 12255232 | tf_op jit(solution)/shard_map/all_gather | solution.py:217
  118.1 3.6 collective-permute-start.11
  119.4 3.7 collective-permute-start.10
  120.7 61.9 %copy-start.24 = (bf16[256]{0:T(256)(128)(2,1)S(1)}, bf16[256]{0:T(256)(128)(2,1)}, u32[]{:S(2)}) copy-start(bf16[256]{0:T(256)(128)(2,1)} %param.24) | copy-start | bytes 1540
  121.8 13.1 %collective-permute-start.13 = (bf16[4,128,256]{2,1,0:T(8,128)(2,1)S(1)}, bf16[4,128,256]{2,1,0:T(8,128)(2,1)S(1)}, u32[]{:S(2)}, u32[]{:S(2)}) collective-permute-start(bf16[4,128,256]{2,1,0:T(8,128)(2,1)S(1)} %fusion.10), channel_id=1, source_target_pairs={{2,0},{4,2},{6,4},{8,6},{10,8},{12,10},{14,12},{16,14},{18,16},{20... | collective-permute-start | bytes 786440 | tf_op jit(solution)/shard_map/ppermute | solution.py:130
  124.2 9.7 %collective-permute-start.12 = (f32[5,128]{1,0:T(8,128)S(1)}, f32[5,128]{1,0:T(8,128)S(1)}, u32[]{:S(2)}, u32[]{:S(2)}) collective-permute-start(f32[5,128]{1,0:T(8,128)S(1)} %concatenate.42), channel_id=1, source_target_pairs={{2,0},{4,2},{6,4},{8,6},{10,8},{12,10},{14,12},{16,14},{18,16},{20... | collective-permute-start | bytes 7688 | tf_op jit(solution)/shard_map/ppermute | solution.py:130
  135.8 19.4 %collective-permute-start.15 = (bf16[4,128,256]{2,1,0:T(8,128)(2,1)}, bf16[4,128,256]{2,1,0:T(8,128)(2,1)S(1)}, u32[]{:S(2)}, u32[]{:S(2)}) collective-permute-start(bf16[4,128,256]{2,1,0:T(8,128)(2,1)} %fusion.14), channel_id=1, source_target_pairs={{4,0},{6,2},{8,4},{10,6},{12,8},{14,10},{16,12},{18,14},{20,16},{2... | collective-permute-start | bytes 786440 | tf_op jit(solution)/shard_map/ppermute | solution.py:130
  137.1 16.9 %collective-permute-start.14 = (f32[5,128]{1,0:T(8,128)S(1)}, f32[5,128]{1,0:T(8,128)S(1)}, u32[]{:S(2)}, u32[]{:S(2)}) collective-permute-start(f32[5,128]{1,0:T(8,128)S(1)} %concatenate.43), channel_id=1, source_target_pairs={{4,0},{6,2},{8,4},{10,6},{12,8},{14,10},{16,12},{18,14},{20,16},{2... | collective-permute-start | bytes 7688 | tf_op jit(solution)/shard_map/ppermute | solution.py:130
  156.2 21.1 %collective-permute-start.17 = (bf16[4,128,256]{2,1,0:T(8,128)(2,1)}, bf16[4,128,256]{2,1,0:T(8,128)(2,1)}, u32[]{:S(2)}, u32[]{:S(2)}) collective-permute-start(bf16[4,128,256]{2,1,0:T(8,128)(2,1)} %fusion.28), channel_id=1, source_target_pairs={{8,0},{10,2},{12,4},{14,6},{16,8},{18,10},{20,12},{22,14},{24,16},... | collective-permute-start | bytes 786440 | tf_op jit(solution)/shard_map/ppermute | solution.py:130
  157.5 18.6 %collective-permute-start.16 = (f32[5,128]{1,0:T(8,128)S(1)}, f32[5,128]{1,0:T(8,128)S(1)}, u32[]{:S(2)}, u32[]{:S(2)}) collective-permute-start(f32[5,128]{1,0:T(8,128)S(1)} %concatenate.44), channel_id=1, source_target_pairs={{8,0},{10,2},{12,4},{14,6},{16,8},{18,10},{20,12},{22,14},{24,16},... | collective-permute-start | bytes 7688 | tf_op jit(solution)/shard_map/ppermute | solution.py:130
  179.3 35.1 %collective-permute-start.19 = (bf16[4,128,256]{2,1,0:T(8,128)(2,1)}, bf16[4,128,256]{2,1,0:T(8,128)(2,1)}, u32[]{:S(2)}, u32[]{:S(2)}) collective-permute-start(bf16[4,128,256]{2,1,0:T(8,128)(2,1)} %fusion.16), channel_id=1, source_target_pairs={{16,0},{18,2},{20,4},{22,6},{24,8},{26,10},{28,12},{30,14},{17,1},... | collective-permute-start | bytes 786440 | tf_op jit(solution)/shard_map/ppermute | solution.py:130
  180.6 32.6 %collective-permute-start.18 = (f32[5,128]{1,0:T(8,128)S(1)}, f32[5,128]{1,0:T(8,128)S(1)}, u32[]{:S(2)}, u32[]{:S(2)}) collective-permute-start(f32[5,128]{1,0:T(8,128)S(1)} %concatenate.45), channel_id=1, source_target_pairs={{16,0},{18,2},{20,4},{22,6},{24,8},{26,10},{28,12},{30,14},{17,1},... | collective-permute-start | bytes 7688 | tf_op jit(solution)/shard_map/ppermute | solution.py:130
  239.1 47.9 %copy-start.14 = (bf16[2048]{0:T(1024)(128)(2,1)S(1)}, bf16[2048]{0:T(1024)(128)(2,1)}, u32[]{:S(2)}) copy-start(bf16[2048]{0:T(1024)(128)(2,1)} %param.26) | copy-start | bytes 12292
  239.1 26.1 %collective-permute-start.21 = (bf16[256,2048]{1,0:T(8,128)(2,1)S(1)}, bf16[256,2048]{1,0:T(8,128)(2,1)S(1)}, u32[]{:S(2)}, u32[]{:S(2)}) collective-permute-start(bf16[256,2048]{1,0:T(8,128)(2,1)S(1)} %convolution_convert_fusion.4), channel_id=1, source_target_pairs={{0,1},{1,0},{2,3},{3,2},{4,5},{5,4},{6,7},{7,6},{8,9},{9,8},{10,11... | collective-permute-start | bytes 3145736 | tf_op jit(solution)/shard_map/ppermute | solution.py:236
  241.9 45.0 %collective-permute-start.20 = (bf16[256,2048]{1,0:T(8,128)(2,1)S(1)}, bf16[256,2048]{1,0:T(8,128)(2,1)S(1)}, u32[]{:S(2)}, u32[]{:S(2)}) collective-permute-start(bf16[256,2048]{1,0:T(8,128)(2,1)S(1)} %convolution_convert_fusion.5), channel_id=1, source_target_pairs={{0,1},{1,0},{2,3},{3,2},{4,5},{5,4},{6,7},{7,6},{8,9},{9,8},{10,11... | collective-permute-start | bytes 3145736 | tf_op jit(solution)/shard_map/ppermute | solution.py:236
  297.2 26.0 %collective-permute-start.23 = (bf16[256,2048]{1,0:T(8,128)(2,1)S(1)}, bf16[256,2048]{1,0:T(8,128)(2,1)S(1)}, u32[]{:S(2)}, u32[]{:S(2)}) collective-permute-start(bf16[256,2048]{1,0:T(8,128)(2,1)S(1)} %get-tuple-element.43), channel_id=1, source_target_pairs={{0,1},{1,0},{2,3},{3,2},{4,5},{5,4},{6,7},{7,6},{8,9},{9,8},{10,11... | collective-permute-start | bytes 3145736 | tf_op jit(solution)/shard_map/ppermute | solution.py:236
  298.6 45.4 %collective-permute-start.22 = (bf16[256,2048]{1,0:T(8,128)(2,1)S(1)}, bf16[256,2048]{1,0:T(8,128)(2,1)S(1)}, u32[]{:S(2)}, u32[]{:S(2)}) collective-permute-start(bf16[256,2048]{1,0:T(8,128)(2,1)S(1)} %get-tuple-element.44), channel_id=1, source_target_pairs={{0,1},{1,0},{2,3},{3,2},{4,5},{5,4},{6,7},{7,6},{8,9},{9,8},{10,11... | collective-permute-start | bytes 3145736 | tf_op jit(solution)/shard_map/ppermute | solution.py:236
  396.9 47.9 %copy-start.10 = (f32[256,2048]{1,0:T(8,128)S(1)}, f32[256,2048]{1,0:T(8,128)}, u32[]{:S(2)}) copy-start(f32[256,2048]{1,0:T(8,128)} %copy-done.9) | copy-start | bytes 6291460
  396.9 26.1 %collective-permute-start.24 = (bf16[256,2048]{1,0:T(8,128)(2,1)S(1)}, bf16[256,2048]{1,0:T(8,128)(2,1)S(1)}, u32[]{:S(2)}, u32[]{:S(2)}) collective-permute-start(bf16[256,2048]{1,0:T(8,128)(2,1)S(1)} %convolution_convert_fusion.2), channel_id=1, source_target_pairs={{0,1},{1,0},{2,3},{3,2},{4,5},{5,4},{6,7},{7,6},{8,9},{9,8},{10,11... | collective-permute-start | bytes 3145736 | tf_op jit(solution)/shard_map/ppermute | solution.py:236
  398.5 46.3 %collective-permute-start.25 = (bf16[256,2048]{1,0:T(8,128)(2,1)S(1)}, bf16[256,2048]{1,0:T(8,128)(2,1)S(1)}, u32[]{:S(2)}, u32[]{:S(2)}) collective-permute-start(bf16[256,2048]{1,0:T(8,128)(2,1)S(1)} %convolution_convert_fusion.1), channel_id=1, source_target_pairs={{0,1},{1,0},{2,3},{3,2},{4,5},{5,4},{6,7},{7,6},{8,9},{9,8},{10,11... | collective-permute-start | bytes 3145736 | tf_op jit(solution)/shard_map/ppermute | solution.py:236
  (30 other events, 272.9 us)
Sparse Core Ops, SparseCore 0:
  9.6 105.0 all-gather.3
  118.2 121.0 all-gather.5
  287.0 98.2 all-gather.7
where the time goes:
time: 461 us; the launch traced here: 454 us
  waiting for transfers between devices  213 us (46%)
  starting transfers between devices  94.1 us (20%)
  matrix products  64.7 us (14%)
  Pallas kernels  22.7 us (5%)
  between operations  21.7 us (5%)
  local copies, waits for them, and re-layouts  19.3 us (4%)
  other arithmetic  18.9 us (4%)
    ppermute x6, waiting for transfers between devices, per_device(): swap = lambda x: lax.ppermute(x, 'tp', [(0, 1), (1, 0)])  107 us
    ppermute x20, starting transfers between devices, from_away(): return (lax.ppermute(state, 'sp', pairs), lax.ppermute(small, 'sp', pairs))  87.8 us
    ppermute x20, waiting for transfers between devices, from_away(): return (lax.ppermute(state, 'sp', pairs), lax.ppermute(small, 'sp', pairs))  82.4 us
    dot_general x13, matrix products, product(): return jnp.dot(a, b, preferred_element_type=jnp.float32)  64.7 us
    all_gather x3, waiting for transfers between devices, per_device(): gather = lambda w, axis: lax.all_gather(w, 'sp', axis=axis, tiled=True)  23.1 us
    pallas_call x1, Pallas kernels, attention(): pl.pallas_call(functools.partial(head_outputs, blocks, size), grid=(heads...  17.8 us
    unnamed x67, local copies, waits for them, and re-layouts  9.99 us
  transfers between devices with their start and end apart: 29, of which 16 were waited for; matrix products, arithmetic and copies ran while one was open for 18% of the time, Pallas kernels for 5%

commit v1 on v0

--- a/solution.py
+++ b/solution.py
@@ -210,10 +210,711 @@
     return mixed, up_weight, gate_full
 
 
+MESH = pl.DeviceIdType.MESH
+Z1, Z2, Z3, YY, SS = 4, 8, 12, 2, 1
+FIRST, LAST = 4, 5
+WIDE = 256
+
+
+class Net:
+    def __init__(self, planes):
+        place = lax.axis_index("sp")
+        self.t = lax.axis_index("tp")
+        self.c = place % 2
+        self.y = (place // 2) % 2
+        self.z = place // 4
+        z = self.z
+        self.zs = [z, z + 1 - 2 * (z % 2), (z + 2) % planes, planes - 1 - z]
+        self.ys = [self.y, 1 - self.y]
+        self.cs = [self.c, 1 - self.c]
+        self.middle = (z == 1) | (z == 2)
+
+    def chip(self, r):
+        return self.zs[r // 4] * 2 + self.ys[(r // 2) % 2]
+
+    def shard(self, r):
+        return self.chip(r) * 2 + self.cs[r % 2]
+
+    def dev(self, r):
+        return (self.shard(r), self.t)
+
+    def across(self):
+        return (self.shard(0), 1 - self.t)
+
+
+def maybe(cond, do):
+    if cond is None:
+        do()
+    else:
+        pl.when(cond)(do)
+
+
+class Sends:
+    def __init__(self):
+        self.open = []
+
+    def go(self, src, dst, send, recv, device, cond=None):
+        copy = pltpu.make_async_remote_copy(src_ref=src, dst_ref=dst, send_sem=send, recv_sem=recv,
+                                            device_id=device, device_id_type=MESH)
+        maybe(cond, copy.start)
+        self.open.append((copy, cond))
+
+    def settle(self):
+        copy, cond = self.open.pop()
+        return functools.partial(maybe, cond, copy.wait_send)
+
+    def drain(self):
+        for copy, cond in self.open:
+            maybe(cond, copy.wait_send)
+        self.open = []
+
+
+def arrived(ref, sem, cond=None):
+    maybe(cond, pltpu.make_async_copy(ref, ref, sem).wait)
+
+
+class Piece:
+    def __init__(self, net, sends, own, full, recv, send, crossed):
+        self.net, self.sends, self.own, self.full = net, sends, own, full
+        self.recv, self.send, self.crossed, self.count = recv, send, crossed, 0
+
+    def go(self, r, d, cond=None):
+        dst = self.full(self.net.shard(r))
+        self.sends.go(self.own if r == 0 else dst, dst, self.send.at[self.count],
+                      self.recv.at[r ^ d], self.net.dev(d), cond)
+        self.count += 1
+
+    def wait(self, r):
+        arrived(self.full(self.net.shard(r)), self.recv.at[r])
+
+    def along(self, r):
+        self.go(r, Z1)
+        self.go(r, Z2)
+        self.go(r, Z3, self.net.middle)
+
+    def start_y(self):
+        self.go(0, YY)
+
+    def start_z(self):
+        self.along(0)
+
+    def start_s(self):
+        self.go(0, SS)
+
+    def start(self):
+        self.start_y()
+        self.start_z()
+        self.start_s()
+
+    def line(self, a):
+        r = a * 4
+        self.wait(r)
+        if a == 2:
+            self.go(r, Z1, self.net.middle)
+        if not self.crossed:
+            self.go(r, YY)
+        self.go(r, SS)
+
+    def beside(self, a):
+        r = a * 4 + YY
+        self.wait(r)
+        if self.crossed:
+            if a == 0:
+                self.along(r)
+            if a == 2:
+                self.go(r, Z1, self.net.middle)
+        self.go(r, SS)
+
+    def near(self):
+        for a in (1, 2):
+            self.line(a)
+            if self.crossed:
+                self.beside(a)
+
+    def far(self):
+        self.line(3)
+        if self.crossed:
+            self.beside(3)
+
+    def hand_over(self):
+        for a in (0, 1, 2, 3):
+            self.beside(a)
+
+    def siblings(self):
+        for a in range(4):
+            for b in range(2):
+                self.sibling(a, b)
+
+    def sibling(self, a, b):
+        self.wait(a * 4 + b * 2 + 1)
+
+
+def column(rows, h):
+    return jnp.transpose(rows)[:, h : h + 1]
+
+
+def prefix_sums(blocks, size, h, decay, table):
+    rows = lax.broadcasted_iota(jnp.int32, (size, size), 0)
+    cols = lax.broadcasted_iota(jnp.int32, (size, size), 1)
+    lower = (cols <= rows).astype(jnp.float32)
+    total = jnp.zeros((1, decay.shape[2]), jnp.float32)
+    for b in range(blocks):
+        here = pl.ds(b * size, size)
+        cum = jnp.dot(lower, decay[h, here, :], precision=HIGH, preferred_element_type=jnp.float32)
+        decay[h, here, :] = cum
+        total = total + cum[size - 1 : size]
+    table[0, pl.ds(h, 1), :] = total
+
+
+def own_states(blocks, size, h, q, k, v, cums, doc, table, onward, rearward, tail, lead, states):
+    scale = q.shape[2] ** (-0.5)
+    total = table[0, pl.ds(h, 1), :]
+    first = doc[0:1, :]
+    last = doc[blocks * size - 1 : blocks * size, :]
+    before = jnp.zeros_like(total)
+    for b in range(blocks):
+        here = pl.ds(b * size, size)
+        inner = cums[h, here, :]
+        cum = inner + before
+        before = before + inner[size - 1 : size]
+        keys = k[h, here, :].astype(jnp.float32)
+        query = q[h, here, :].astype(jnp.float32) * scale
+        docs = doc[here, :]
+        grown = jnp.where(docs == first, jnp.exp(cum), 0.0)
+        shrunk = jnp.where(docs == last, jnp.exp(total - cum), 0.0)
+        tail[here, :] = (keys * shrunk).astype(jnp.bfloat16)
+        lead[here, :] = (keys * grown).astype(jnp.bfloat16)
+        onward[h, here, :] = (query * grown).astype(jnp.bfloat16)
+        rearward[h, here, :] = (query * shrunk).astype(jnp.bfloat16)
+    values = v[h]
+    states[0, h] = lax.dot_general(tail[...], values, TN,
+                                   preferred_element_type=jnp.float32).astype(jnp.bfloat16)
+    states[1, h] = lax.dot_general(lead[...], values, TN,
+                                   preferred_element_type=jnp.float32).astype(jnp.bfloat16)
+
+
+def inner_outputs(blocks, size, h, q, k, v, cums, doc, doc_row, back, out):
+    scale = q.shape[2] ** (-0.5)
+    rows = lax.broadcasted_iota(jnp.int32, (size, size), 0)
+    cols = lax.broadcasted_iota(jnp.int32, (size, size), 1)
+    later = jnp.zeros((k.shape[2], v.shape[2]), jnp.float32)
+    for b in reversed(range(blocks)):
+        here = pl.ds(b * size, size)
+        back[b] = later.astype(jnp.bfloat16)
+        if b:
+            cum = cums[h, here, :]
+            docs = doc[here, :]
+            first, last = docs[0:1], docs[size - 1 : size]
+            previous = doc[b * size - 1 : b * size, :]
+            grown = jnp.where(docs == first, k[h, here, :].astype(jnp.float32) * jnp.exp(cum), 0.0)
+            added = lax.dot_general(grown.astype(jnp.bfloat16), v[h, here, :], TN,
+                                    preferred_element_type=jnp.float32)
+            through = jnp.where(first == last, jnp.exp(cum[size - 1 : size]), 0.0)
+            later = added + jnp.transpose(through) * later
+            later = jnp.where(jnp.transpose(previous == first), later, 0.0)
+    earlier = jnp.zeros((k.shape[2], v.shape[2]), jnp.float32)
+    for b in range(blocks):
+        here = pl.ds(b * size, size)
+        cum = cums[h, here, :]
+        docs = doc[here, :]
+        first, last = docs[0:1], docs[size - 1 : size]
+        end = cum[size - 1 : size]
+        query = q[h, here, :].astype(jnp.float32) * scale
+        keys = k[h, here, :].astype(jnp.float32)
+        values = v[h, here, :]
+        middle = cum[size // 2 - 1 : size // 2]
+        rising = jnp.exp(cum - middle)
+        falling = jnp.exp(middle - cum)
+        forward = lax.dot_general((query * rising).astype(jnp.bfloat16),
+                                  (keys * falling).astype(jnp.bfloat16), NT,
+                                  preferred_element_type=jnp.float32)
+        backward = lax.dot_general((query * falling).astype(jnp.bfloat16),
+                                   (keys * rising).astype(jnp.bfloat16), NT,
+                                   preferred_element_type=jnp.float32)
+        same = docs[:, :size] == doc_row[b : b + 1, :]
+        scores = jnp.where(same & (cols <= rows), forward, 0.0) + jnp.where(
+            same & (cols >= rows), backward, 0.0)
+        total = jnp.dot(scores.astype(jnp.bfloat16), values, preferred_element_type=jnp.float32)
+        shrink = jnp.exp(end - cum)
+        if b:
+            onward = jnp.where(docs == first, query * jnp.exp(cum), 0.0).astype(jnp.bfloat16)
+            total = total + jnp.dot(onward, earlier.astype(jnp.bfloat16),
+                                    preferred_element_type=jnp.float32)
+        if b < blocks - 1:
+            rearward = jnp.where(docs == last, query * shrink, 0.0).astype(jnp.bfloat16)
+            total = total + jnp.dot(rearward, back[b], preferred_element_type=jnp.float32)
+            tail = jnp.where(docs == last, keys * shrink, 0.0)
+            added = lax.dot_general(tail.astype(jnp.bfloat16), values, TN,
+                                    preferred_element_type=jnp.float32)
+            through = jnp.where(first == last, jnp.exp(end), 0.0)
+            following = doc[(b + 1) * size : (b + 1) * size + 1, :]
+            earlier = added + jnp.transpose(through) * earlier
+            earlier = jnp.where(jnp.transpose(last == following), earlier, 0.0)
+        out[h, here, :] = total
+
+
+def finished_head(h, step, onward, rearward, inner, carry, gate, gain, mixed):
+    def some(i, _):
+        here = pl.ds(pl.multiple_of(i * step, step), step)
+        total = inner[h, here, :]
+        total = total + jnp.dot(onward[h, here, :], carry[0, h], preferred_element_type=jnp.float32)
+        total = total + jnp.dot(rearward[h, here, :], carry[1, h],
+                                preferred_element_type=jnp.float32)
+        scaled = total * lax.rsqrt(jnp.mean(total * total, axis=-1, keepdims=True) + EPS)
+        g = gate[h, here, :].astype(jnp.float32)
+        mixed[h, here, :] = (scaled * gain[...] * (g / (1.0 + jnp.exp(-g)))).astype(jnp.bfloat16)
+        return 0
+
+    lax.fori_loop(0, inner.shape[1] // step, some, 0)
+
+
+def layer_kernel(planes, size, pieces,
+                 stream, queries, keys, values, decay, doc_wide, doc_row, out_gate, head_gain,
+                 out_weight, norm_gain, gate_w, up_w, down_w,
+                 result, gate_full, up_full, down_full,
+                 q, k, v, cums, doc, og, onward, rearward, inner, tail, lead, back,
+                 states, table, chip_state, plane_state, chip_carry, from_sib, from_y, from_z, carry,
+                 mixed, mixed_x, weight, normed, resid, rows_in, hidden, narrow, part, part_x,
+                 load_sem, own_sem, table_send, table_recv, state_send, state_recv,
+                 piece_send, piece_recv, mix_send, mix_recv, wo_send, wo_recv, part_send, part_recv,
+                 row_sem, wide_sem, narrow_sem, done_sem):
+    net = Net(planes)
+    sends = Sends()
+    heads, rows, dk = q.shape
+    dv = v.shape[2]
+    blocks = rows // size
+    c, y, z, t = net.c, net.y, net.z, net.t
+    half = out_weight.shape[0]
+    quarter = half // 2
+    share = rows // 2
+
+    loads = []
+    for h in range(heads):
+        group = []
+        for n, (src, dst, width) in enumerate(((decay, cums, dk), (keys, k, dk), (queries, q, dk),
+                                               (values, v, dv), (out_gate, og, dv))):
+            group.append(pltpu.make_async_copy(src.at[:, h * width : (h + 1) * width], dst.at[h],
+                                               load_sem.at[n, h]))
+        loads.append(group)
+    doc_load = pltpu.make_async_copy(doc_wide, doc, load_sem.at[5, 0])
+    doc_load.start()
+    for n in range(4):
+        for h in range(heads):
+            loads[h][n].start()
+    for h in range(heads):
+        loads[h][4].start()
+
+    barrier = pltpu.get_barrier_semaphore()
+    for r in range(1, 4 * planes):
+        pl.semaphore_signal(barrier, inc=1, device_id=net.dev(r), device_id_type=MESH)
+    pl.semaphore_signal(barrier, inc=1, device_id=net.across(), device_id_type=MESH)
+    pl.semaphore_wait(barrier, 4 * planes)
+
+    shards = {"g": (gate_w, gate_full), "u": (up_w, up_full), "d": (down_w, down_full)}
+
+    def place(full, low, high, shard):
+        if len(full.shape) == 3:
+            return full.at[shard, low:high]
+        own = full.shape[0] // (4 * planes)
+        return full.at[pl.ds(pl.multiple_of(shard * own, own), own), low:high]
+
+    ps = []
+    for i, (name, low, high, crossed) in enumerate(pieces):
+        own, full = shards[name]
+        mine = own.at[low:high] if len(full.shape) == 3 else own.at[:, low:high]
+        ps.append(Piece(net, sends, mine, functools.partial(place, full, low, high),
+                        piece_recv.at[i], piece_send.at[i], crossed))
+    gate_a_columns = pieces[0][2]
+    gate_a, up_a, gate_b, up_b, down_a, down_b, cross_a, cross_b = ps
+    gate_a.start()
+    mine_low = pl.multiple_of(t * half, half)
+    away_low = pl.multiple_of((1 - t) * half, half)
+    sends.go(out_weight.at[pl.ds(pl.multiple_of(c * quarter, quarter), quarter)],
+             weight.at[pl.ds(pl.multiple_of(t * half + c * quarter, quarter), quarter)],
+             wo_send.at[0], wo_recv.at[0], net.across())
+    own_copies = [pltpu.make_async_copy(out_weight, weight.at[pl.ds(mine_low, half)], own_sem.at[0])]
+    me = net.shard(0)
+    for i, (own, full) in enumerate(shards.values()):
+        own_copies.append(pltpu.make_async_copy(
+            own, place(full, 0, own.shape[len(full.shape) == 2], me), own_sem.at[i + 1]))
+
+    for h in range(heads):
+        loads[h][0].wait()
+    doc_load.wait()
+    table[0] = jnp.where(
+        lax.broadcasted_iota(jnp.int32, table.shape[1:], 0) == FIRST,
+        jnp.broadcast_to(doc[0:1, :], table.shape[1:]),
+        jnp.broadcast_to(doc[rows - 1 : rows, :], table.shape[1:]))
+
+    def sums(h, _):
+        prefix_sums(blocks, size, h, cums, table)
+        return 0
+
+    lax.fori_loop(0, heads, sums, 0)
+    for h in range(heads):
+        for n in (1, 2, 3):
+            loads[h][n].wait()
+
+    def state_of(h, _):
+        own_states(blocks, size, h, q, k, v, cums, doc, table, onward, rearward, tail, lead, states)
+        return 0
+
+    lax.fori_loop(0, 1, state_of, 0)
+    for r in range(1, 4 * planes):
+        sends.go(table.at[0], table.at[r], table_send.at[r], table_recv.at[r], net.dev(r))
+    lax.fori_loop(1, heads, state_of, 0)
+    sends.go(states.at[c], from_sib, state_send.at[0], state_recv.at[0], net.dev(SS))
+    for copy in own_copies:
+        copy.start()
+
+    def state(r):
+        return table[r]
+
+    rising = c == 1
+
+    def leaves(r):
+        return jnp.where(rising, state(r)[LAST : LAST + 1], state(r)[FIRST : FIRST + 1])
+
+    def enters(r):
+        return jnp.where(rising, state(r)[FIRST : FIRST + 1], state(r)[LAST : LAST + 1])
+
+    def chip_log(r):
+        return state(r) + state(r ^ 1)
+
+    def plane_log(a):
+        return chip_log(a * 4) + chip_log(a * 4 + 2)
+
+    arrived(table.at[1], table_recv.at[1])
+    arrived(from_sib, state_recv.at[0])
+    fade = jnp.where(leaves(1) == leaves(0), jnp.exp(state(0)), 0.0)
+    way = 1 - c
+    for h in range(heads):
+        chip_state[h] = (states[way, h].astype(jnp.float32)
+                         + column(fade, h) * from_sib[h].astype(jnp.float32)).astype(jnp.bfloat16)
+    sends.go(chip_state, from_y, state_send.at[1], state_recv.at[1], net.dev(YY))
+
+    def inner_of(h, _):
+        inner_outputs(blocks, size, h, q, k, v, cums, doc, doc_row, back, inner)
+        return 0
+
+    lax.fori_loop(0, 2, inner_of, 0)
+    for r in range(2, 4 * planes):
+        arrived(table.at[r], table_recv.at[r])
+    arrived(from_y, state_recv.at[1])
+    upper = y == c
+    fade = jnp.where(leaves(2) == leaves(0),
+                     jnp.exp(jnp.where(upper, chip_log(0), chip_log(2))), 0.0)
+    for h in range(heads):
+        mine = chip_state[h].astype(jnp.float32)
+        other = from_y[h].astype(jnp.float32)
+        high = jnp.where(upper, mine, other)
+        low = jnp.where(upper, other, mine)
+        plane_state[h] = (high + column(fade, h) * low).astype(jnp.bfloat16)
+    early, late = [None], [None]
+    for a in range(1, planes):
+        below = net.zs[a] < z
+        early.append((rising & below) | ((c == 0) & (net.zs[a] > z)))
+        late.append((rising & (net.zs[a] > z)) | ((c == 0) & below))
+    for a in range(1, planes):
+        sends.go(plane_state, from_z.at[a - 1], state_send.at[1 + a], state_recv.at[1 + a],
+                 net.dev(a * 4), late[a])
+    up_a.start_y()
+    up_a.start_s()
+    lax.fori_loop(2, heads, inner_of, 0)
+    up_a.start_z()
+    gate_a.near()
+    for a in range(1, planes):
+        arrived(from_z.at[a - 1], state_recv.at[1 + a], early[a])
+    entry = enters(1)
+    fades = []
+    for a in range(1, planes):
+        log = jnp.where(upper, chip_log(2), 0.0)
+        for b in range(1, planes):
+            if b != a:
+                between = (net.zs[b] - net.zs[a]) * (z - net.zs[b]) > 0
+                log = log + jnp.where(between, plane_log(b), 0.0)
+        out_doc = jnp.where(upper, leaves(a * 4), leaves(a * 4 + 2))
+        fades.append(jnp.where((out_doc == entry) & early[a], jnp.exp(log), 0.0))
+    joins = jnp.where((leaves(2) == entry) & upper, jnp.ones_like(entry), 0.0)
+    joins = jnp.broadcast_to(joins, (8, dk))
+    through = jnp.where(enters(1) == leaves(1), jnp.exp(state(1)), 0.0)
+    joined = jnp.broadcast_to(jnp.where(leaves(1) == enters(0), jnp.ones_like(entry), 0.0), (8, dk))
+    for h in range(heads):
+        into = column(joins, h) * from_y[h].astype(jnp.float32)
+        for a in range(1, planes):
+            into = into + column(fades[a - 1], h) * jnp.where(
+                early[a], from_z[a - 1, h].astype(jnp.float32), 0.0)
+        chip_carry[h] = into.astype(jnp.bfloat16)
+        carry[way, h] = (column(joined, h) * (from_sib[h].astype(jnp.float32)
+                                              + column(through, h) * into)).astype(jnp.bfloat16)
+    sends.go(chip_carry, carry.at[way], state_send.at[5], state_recv.at[5], net.dev(SS))
+    own_part = weight.at[pl.ds(pl.multiple_of((1 - t) * half + c * quarter, quarter), quarter)]
+    sib_part = weight.at[pl.ds(pl.multiple_of((1 - t) * half + (1 - c) * quarter, quarter), quarter)]
+    arrived(own_part, wo_recv.at[0])
+    sends.go(own_part, own_part, wo_send.at[1], wo_recv.at[1], net.dev(SS))
+    weight_sent = sends.settle()
+    for h in range(heads):
+        loads[h][4].wait()
+    arrived(carry.at[c], state_recv.at[5])
+    for h in range(heads):
+        finished_head(h, 256, onward, rearward, inner, carry, og, head_gain, mixed)
+        if h:
+            sends.go(mixed.at[h - 1], mixed_x.at[h - 1], mix_send.at[h - 1], mix_recv.at[h - 1],
+                     net.across())
+    own_copies[0].wait()
+    sends.go(mixed.at[heads - 1], mixed_x.at[heads - 1], mix_send.at[heads - 1],
+             mix_recv.at[heads - 1], net.across())
+    gate_a.far()
+    gate_b.start()
+
+    step = rows_in.shape[1]
+    steps = rows // step
+
+    def row_load(i, slot):
+        return pltpu.make_async_copy(stream.at[pl.ds(pl.multiple_of(i * step, step), step)],
+                                     rows_in.at[slot], row_sem.at[slot])
+
+    def all_heads(ref, here):
+        return jnp.concatenate([ref[h, here, :] for h in range(heads)], axis=1)
+
+    def own_product(i, _):
+        here = pl.ds(pl.multiple_of(i * step, step), step)
+        normed[here, :] = product(all_heads(mixed, here),
+                                  weight[pl.ds(mine_low, half), :]).astype(jnp.bfloat16)
+        return 0
+
+    row_load(0, 0).start()
+    lax.fori_loop(0, steps, own_product, 0)
+    up_a.near()
+    cross_a.start()
+    up_a.far()
+    gate_a.hand_over()
+    up_b.start()
+    gate_b.near()
+    cross_a.beside(0)
+    up_a.hand_over()
+    gate_b.far()
+    cross_b.start()
+    for h in range(heads):
+        arrived(mixed_x.at[h], mix_recv.at[h])
+    arrived(sib_part, wo_recv.at[1])
+
+    def attend(i, _):
+        slot = i % 2
+        row_load(i, slot).wait()
+
+        @pl.when(i + 1 < steps)
+        def _():
+            row_load(i + 1, 1 - slot).start()
+
+        here = pl.ds(pl.multiple_of(i * step, step), step)
+        away = product(all_heads(mixed_x, here),
+                       weight[pl.ds(away_low, half), :]).astype(jnp.bfloat16)
+        total = rows_in[slot].astype(jnp.float32) + (
+            normed[here, :].astype(jnp.float32) + away.astype(jnp.float32))
+        per = share // step
+
+        @pl.when(i // per == t)
+        def _():
+            there = pl.ds(pl.multiple_of((i % per) * step, step), step)
+            for n in range(resid.shape[0]):
+                resid[n, there, :] = total[:, n * WIDE : (n + 1) * WIDE]
+
+        factor = lax.rsqrt(jnp.mean(total * total, axis=-1, keepdims=True) + EPS)
+        normed[here, :] = (total * factor * norm_gain[...]).astype(jnp.bfloat16)
+        return 0
+
+    lax.fori_loop(0, steps, attend, 0)
+    cross_a.near()
+    up_b.near()
+    cross_b.beside(0)
+    down_a.start()
+    own_copies[1].wait()
+    own_copies[2].wait()
+    gate_a.siblings()
+    up_a.siblings()
+
+    columns = hidden.shape[1] // WIDE
+
+    def wide_at(slot, n):
+        return pl.ds(pl.multiple_of((slot * 2 + n) * WIDE, WIDE), WIDE)
+
+    def wide_load(j, slot):
+        there = pl.ds(pl.multiple_of(j * WIDE, WIDE), WIDE)
+        return [pltpu.make_async_copy(full.at[:, there], weight.at[:, wide_at(slot, n)],
+                                      wide_sem.at[slot, n])
+                for n, full in enumerate((gate_full, up_full))]
+
+    def hidden_block(end, j, _):
+        slot = j % 2
+        for copy in wide_load(j, slot):
+            copy.wait()
+
+        @pl.when(j + 1 < end)
+        def _():
+            for copy in wide_load(j + 1, 1 - slot):
+                copy.start()
+
+        there = pl.ds(pl.multiple_of(j * WIDE, WIDE), WIDE)
+
+        def some(i, _):
+            here = pl.ds(pl.multiple_of(i * share, share), share)
+            g = product(normed[here, :], weight[:, wide_at(slot, 0)])
+            u = product(normed[here, :], weight[:, wide_at(slot, 1)])
+            hidden[here, there] = (g / (1.0 + jnp.exp(-g)) * u).astype(jnp.bfloat16)
+            return 0
+
+        lax.fori_loop(0, 2, some, 0)
+        return 0
+
+    def hidden_blocks(begin, end):
+        for copy in wide_load(begin, begin % 2):
+            copy.start()
+        lax.fori_loop(begin, end, functools.partial(hidden_block, end), 0)
+
+    weight_sent()
+    cut = gate_a_columns // WIDE
+    hidden_blocks(0, cut)
+    up_b.far()
+    cross_a.far()
+    down_b.start()
+    gate_b.hand_over()
+    up_b.hand_over()
+    cross_b.near()
+    down_a.near()
+    gate_b.siblings()
+    up_b.siblings()
+    hidden_blocks(cut, columns)
+    down_b.near()
+    cross_b.far()
+    own_copies[3].wait()
+    downs = (down_a, down_b, cross_a, cross_b)
+
+    order = [(a, b) for a in range(planes) for b in range(2)]
+    lanes = narrow.shape[2] // 2
+    here = pl.ds(pl.multiple_of(t * share, share), share)
+    there = pl.ds(pl.multiple_of((1 - t) * share, share), share)
+
+    def narrow_load(n):
+        pair = net.chip(order[n][0] * 4 + order[n][1] * 2) * 2
+        return [pltpu.make_async_copy(down_full.at[pair + m],
+                                      narrow.at[n % 2, :, m * lanes : (m + 1) * lanes],
+                                      narrow_sem.at[n % 2, m]) for m in range(2)]
+
+    for a in range(planes):
+        if a == 3:
+            down_a.far()
+            down_b.far()
+        down_a.beside(a)
+        down_b.beside(a)
+        for b in range(2):
+            for p in downs:
+                p.sibling(a, b)
+            for copy in narrow_load(a * 2 + b):
+                copy.start()
+        for b in range(2):
+            n = a * 2 + b
+            for copy in narrow_load(n):
+                copy.wait()
+            part[n] = product(hidden[there, :], narrow[b]).astype(jnp.bfloat16)
+            kept = product(hidden[here, :], narrow[b]).astype(jnp.bfloat16)
+            sends.go(part.at[n], part_x.at[n], part_send.at[n], part_recv.at[n], net.across())
+            block = net.chip(a * 4 + b * 2)
+            resid[block] = resid[block] + kept.astype(jnp.float32)
+    outs = []
+    for n in range(len(order)):
+        block = net.chip(order[n][0] * 4 + order[n][1] * 2)
+        arrived(part_x.at[n], part_recv.at[n])
+        part_x[n] = (resid[block] + part_x[n].astype(jnp.float32)).astype(jnp.bfloat16)
+        out = pltpu.make_async_copy(
+            part_x.at[n], result.at[:, pl.ds(pl.multiple_of(block * WIDE, WIDE), WIDE)], done_sem.at[n])
+        out.start()
+        outs.append(out)
+    for out in outs:
+        out.wait()
+    sends.drain()
+
+
+def pieces_of(units):
+    half = (units // WIDE + 1) // 2 * WIDE
+    pieces = [(w, a, b, False) for a, b in ((0, half), (half, units)) for w in "gu"]
+    return pieces + [("d", units * i // 4, units * (i + 1) // 4, i >= 2) for i in range(4)]
+
+
+def whole_layer(stream, queries, projected_keys, values, decay_gate_logits, decay_gate_bias,
+                extra_log_decay, document_index, output_gate, head_norm_gain, output_weight,
+                feedforward_norm_gain, gate_weight, up_weight, down_weight):
+    heads = extra_log_decay.shape[1]
+    rows, width = stream.shape
+    dk = queries.shape[1] // heads
+    dv = values.shape[1] // heads
+    size = BLOCK_LENGTH
+    blocks = rows // size
+    devices = lax.axis_size("sp")
+    planes = devices // 4
+    share = rows // 2
+    units = gate_weight.shape[1]
+    chips = devices // 2
+    decay = jax.nn.log_sigmoid(decay_gate_logits.astype(jnp.float32) + decay_gate_bias) / TAU
+    decay = (decay.reshape(rows, heads, dk) + extra_log_decay[:, :, None]).reshape(rows, -1)
+    doc = document_index.astype(jnp.float32)
+    doc_wide = jnp.broadcast_to(doc[:, None], (rows, dk))
+    doc_row = doc.reshape(blocks, size)
+    pieces = pieces_of(units)
+    any_, vm = pl.BlockSpec(memory_space=pl.ANY), pl.BlockSpec(memory_space=pltpu.VMEM)
+    b16, f32 = jnp.bfloat16, jnp.float32
+    dma = pltpu.SemaphoreType.DMA
+    state = (heads, dk, dv)
+    step = 256
+    scratch = [
+        pltpu.VMEM((heads, rows, dk), b16), pltpu.VMEM((heads, rows, dk), b16),
+        pltpu.VMEM((heads, rows, dv), b16), pltpu.VMEM((heads, rows, dk), f32),
+        pltpu.VMEM((rows, dk), f32), pltpu.VMEM((heads, rows, dv), b16),
+        pltpu.VMEM((heads, rows, dk), b16), pltpu.VMEM((heads, rows, dk), b16),
+        pltpu.VMEM((heads, rows, dv), f32), pltpu.VMEM((rows, dk), b16), pltpu.VMEM((rows, dk), b16),
+        pltpu.VMEM((blocks, dk, dv), b16),
+        pltpu.VMEM((2,) + state, b16), pltpu.VMEM((devices, 8, dk), f32),
+        pltpu.VMEM(state, b16), pltpu.VMEM(state, b16), pltpu.VMEM(state, b16),
+        pltpu.VMEM(state, b16), pltpu.VMEM(state, b16), pltpu.VMEM((planes - 1,) + state, b16),
+        pltpu.VMEM((2,) + state, b16),
+        pltpu.VMEM((heads, rows, dv), b16), pltpu.VMEM((heads, rows, dv), b16),
+        pltpu.VMEM((2 * output_weight.shape[0], width), b16), pltpu.VMEM((rows, width), b16),
+        pltpu.VMEM((chips, share, WIDE), f32), pltpu.VMEM((2, step, width), b16),
+        pltpu.VMEM((rows, units), b16),
+        pltpu.VMEM((2, units, WIDE), b16), pltpu.VMEM((chips, share, WIDE), b16),
+        pltpu.VMEM((chips, share, WIDE), b16),
+        dma((6, heads)), dma((4,)), dma((devices,)), dma((devices,)), dma((8,)), dma((8,)),
+        dma((len(pieces), 24)), dma((len(pieces), devices)), dma((heads,)), dma((heads,)),
+        dma((2,)), dma((2,)), dma((chips,)), dma((chips,)), dma((2,)), dma((2, 2)), dma((2, 2)),
+        dma((chips,)),
+    ]
+    result = pl.pallas_call(
+        functools.partial(layer_kernel, planes, size, pieces),
+        out_shape=[
+            jax.ShapeDtypeStruct(shape, b16)
+            for shape in ((share, width), (devices * gate_weight.shape[0], units),
+                          (devices * up_weight.shape[0], units), (devices,) + down_weight.shape)],
+        in_specs=[any_] * 6 + [vm, any_, vm, any_, vm, any_, any_, any_],
+        out_specs=[any_] * 4,
+        scratch_shapes=scratch,
+        compiler_params=pltpu.CompilerParams(collective_id=0, has_side_effects=True,
+                                             vmem_limit_bytes=67043328),
+        name="whole_layer",
+    )(stream, queries, projected_keys, values, decay, doc_wide, doc_row, output_gate,
+      head_norm_gain.astype(f32)[None], output_weight, feedforward_norm_gain.astype(f32)[None],
+      gate_weight, up_weight, down_weight)
+    return result[0]
+
+
 def per_device(stream, queries, projected_keys, values, decay_gate_logits, decay_gate_bias,
                extra_log_decay, document_index, output_gate, head_norm_gain, output_weight,
                feedforward_norm_gain, gate_weight, up_weight, down_weight):
     tp = lax.axis_size("tp")
+    if tp == 2 and lax.axis_size("sp") == 16:
+        return whole_layer(
+            stream, queries, projected_keys, values, decay_gate_logits, decay_gate_bias,
+            extra_log_decay, document_index, output_gate, head_norm_gain, output_weight,
+            feedforward_norm_gain, gate_weight, up_weight, down_weight)
     gather = lambda w, axis: lax.all_gather(w, "sp", axis=axis, tiled=True)
     gate_full = gather(gate_weight, 0)
     mixed, up_weight, gate_full = attention(

time: 461 us -> 265 us (0.57); the launches traced: 454 us -> 265 us
  Pallas kernels: 22.7 us -> 251 us
  waiting for transfers between devices: 213 us -> 0 us
  starting transfers between devices: 94.1 us -> 0 us
  matrix products: 64.7 us -> 0 us
  between operations: 21.7 us -> 0.05 us
  other arithmetic: 18.9 us -> 6.03 us
  local copies, waits for them, and re-layouts: 19.3 us -> 6.98 us
    pallas_call x2 -> x1, Pallas kernels: 22.7 us -> 251 us  [whole_layer(): pl.pallas_call(functools.partial(layer_kernel, planes, size, pieces), out...]
    ppermute x26 -> x0, waiting for transfers between devices: 189 us -> none  [the longest x6 107 us: per_device(): swap = lambda x: lax.ppermute(x, 'tp', [(0, 1), (1, 0)])]
    ppermute x26 -> x0, starting transfers between devices: 94 us -> none  [the longest x20 87.8 us: from_away(): return (lax.ppermute(state, 'sp', pairs), lax.ppermute(small, 'sp', pairs))]
    dot_general x13 -> x0, matrix products: 64.7 us -> none  [product(): return jnp.dot(a, b, preferred_element_type=jnp.float32)]
    all_gather x3 -> x0, waiting for transfers between devices: 23.1 us -> none  [per_device(): gather = lambda w, axis: lax.all_gather(w, 'sp', axis=axis, tiled=True)]
    convert_element_type x15 -> x1, other arithmetic: 12.4 us -> 0.69 us  [whole_layer(): doc = document_index.astype(jnp.float32)]
    unnamed x67 -> x6, local copies, waits for them, and re-layouts: 9.99 us -> 4.1 us
    slice x12 -> x0, local copies, waits for them, and re-layouts: 5.69 us -> none  [the longest x8 4.13 us: carried_in(): reach = (place > distance) & (small[-1, 0] == document)]
  transfers between devices with their start and end apart: 29 -> 0, of which waited for: 16 -> 0; matrix products, arithmetic and copies ran while one was open for 18% -> 0% of each run, Pallas kernels for 5% -> 0%
where the time goes in v1:
time: 265 us
  Pallas kernels  251 us (95%)
  local copies, waits for them, and re-layouts  6.98 us (3%)
  other arithmetic  6.03 us (2%)
    pallas_call x1, Pallas kernels, whole_layer(): pl.pallas_call(functools.partial(layer_kernel, planes, size, pieces), out...  251 us

profile of v1, /device:TPU:0, one launch (start us, length us, event | category | flops | bytes accessed | tf_op | source)
XLA Modules:
  0.0 264.6 jit_solution(1795854727335697)
XLA Ops:
  0.0 0.0 copy-start.1
  0.0 0.0 copy-start
  0.0 1.3 broadcast_in_dim.23
  1.3 0.7 convert_element_type.9
  2.0 0.7 reshape.9.doc_row
  2.7 1.3 broadcast_in_dim.24
  4.0 1.0 broadcast_in_dim.18.doc_wide
  4.9 0.9 copy.16
  5.9 1.2 add.27
  7.1 0.0 copy-done.1
  7.1 0.0 copy-done
  7.1 2.7 %fusion.2.decay = f32[1024,512]{1,0:T(8,128)} fusion(f32[128,8,4,128]{3,2,1,0:T(4,128)S(1)} %bitcast.5, bf16[1024,512]{1,0:T(8,128)(2,1)S(1)} %copy-done, f32[512]{0:T(512)S(1)} %copy-done.1), kind=kLoop, calls=%fused_computation.3 | loop fusion | flops 6291456 | bytes 5244928 | tf_op jit(solution)/shard_map/add | solution.py:859
  9.9 251.5 %whole_layer.1 = (bf16[512,2048]{1,0:T(8,128)(2,1)}, bf16[2048,2816]{1,0:T(8,128)(2,1)}, bf16[2048,2816]{1,0:T(8,128)(2,1)}, bf16[16,2816,128]{2,1,0:T(8,128)(2,1)}) custom-call(bf16[1024,2048]{1,0:T(8,128)(2,1)} %stream.1, bf16[1024,512]{1,0:T(8,128)(2,1)} %queries.1, bf16[1024,512]{1,0:T(8,128)(2,1)} %keys.1, bf16[1024,1024]{1,0:T(8,128)(2,1)} %values.1, ...), custom_call_target="tpu_custom_call" | custom-call | tf_op jit(solution)/shard_map/whole_layer/pallas_call | solution.py:891
  261.4 3.2 %copy.20 = bf16[512,2048]{1,0:T(8,128)(2,1)} copy(bf16[512,2048]{1,0:T(8,128)(2,1)} %get-tuple-element.6) | data formatting | bytes 4194304
Async XLA Ops:
  0.0 7.1 %copy-start.1 = (f32[512]{0:T(512)S(1)}, f32[512]{0:T(512)}, u32[]{:S(2)}) copy-start(f32[512]{0:T(512)} %param.20) | copy-start | bytes 6148
  0.0 7.1 %copy-start = (bf16[1024,512]{1,0:T(8,128)(2,1)S(1)}, bf16[1024,512]{1,0:T(8,128)(2,1)}, u32[]{:S(2)}) copy-start(bf16[1024,512]{1,0:T(8,128)(2,1)} %param.19) | copy-start | bytes 3145732

commit v2 on v1

--- a/solution.py
+++ b/solution.py
@@ -294,17 +294,10 @@
 
     def start_y(self):
         self.go(0, YY)
+        self.go(0, SS)
 
     def start_z(self):
         self.along(0)
-
-    def start_s(self):
-        self.go(0, SS)
-
-    def start(self):
-        self.start_y()
-        self.start_z()
-        self.start_s()
 
     def line(self, a):
         r = a * 4
@@ -325,21 +318,6 @@
                 self.go(r, Z1, self.net.middle)
         self.go(r, SS)
 
-    def near(self):
-        for a in (1, 2):
-            self.line(a)
-            if self.crossed:
-                self.beside(a)
-
-    def far(self):
-        self.line(3)
-        if self.crossed:
-            self.beside(3)
-
-    def hand_over(self):
-        for a in (0, 1, 2, 3):
-            self.beside(a)
-
     def siblings(self):
         for a in range(4):
             for b in range(2):
@@ -353,15 +331,31 @@
     return jnp.transpose(rows)[:, h : h + 1]
 
 
-def prefix_sums(blocks, size, h, decay, table):
+def document_columns(blocks, size, doc_line, doc, doc_row):
+    rows = lax.broadcasted_iota(jnp.int32, (size, size), 0)
+    cols = lax.broadcasted_iota(jnp.int32, (size, size), 1)
+    for b in range(blocks):
+        line = doc_line[0:1, b * size : (b + 1) * size].astype(jnp.float32)
+        doc_row[b : b + 1, :] = line
+        column = jnp.sum(jnp.where(rows == cols, line, 0.0), axis=1, keepdims=True)
+        doc[pl.ds(b * size, size), :] = jnp.broadcast_to(column, (size, doc.shape[1]))
+
+
+def prefix_sums(blocks, size, h, logits, bias, extra, cums, table):
     rows = lax.broadcasted_iota(jnp.int32, (size, size), 0)
     cols = lax.broadcasted_iota(jnp.int32, (size, size), 1)
     lower = (cols <= rows).astype(jnp.float32)
-    total = jnp.zeros((1, decay.shape[2]), jnp.float32)
+    total = jnp.zeros((1, cums.shape[2]), jnp.float32)
+    shift = bias[pl.ds(h, 1), :]
+    line = extra[pl.ds(h, 1), :]
     for b in range(blocks):
         here = pl.ds(b * size, size)
-        cum = jnp.dot(lower, decay[h, here, :], precision=HIGH, preferred_element_type=jnp.float32)
-        decay[h, here, :] = cum
+        x = logits[h, here, :].astype(jnp.float32) + shift
+        decay = (jnp.minimum(x, 0.0) - jnp.log1p(jnp.exp(-jnp.abs(x)))) / TAU
+        added = line[:, b * size : (b + 1) * size]
+        cum = jnp.dot(lower, decay, precision=HIGH, preferred_element_type=jnp.float32)
+        cum = cum + jnp.sum(lower * added, axis=1, keepdims=True)
+        cums[h, here, :] = cum
         total = total + cum[size - 1 : size]
     table[0, pl.ds(h, 1), :] = total
 
@@ -468,13 +462,13 @@
     lax.fori_loop(0, inner.shape[1] // step, some, 0)
 
 
-def layer_kernel(planes, size, pieces,
-                 stream, queries, keys, values, decay, doc_wide, doc_row, out_gate, head_gain,
+def layer_kernel(planes, size, pieces, plan, groups,
+                 stream, queries, keys, values, logits_w, bias, extra, doc_line, out_gate, head_gain,
                  out_weight, norm_gain, gate_w, up_w, down_w,
                  result, gate_full, up_full, down_full,
-                 q, k, v, cums, doc, og, onward, rearward, inner, tail, lead, back,
+                 q, k, v, logits, cums, doc, doc_row, og, onward, rearward, inner, tail, lead, back,
                  states, table, chip_state, plane_state, chip_carry, from_sib, from_y, from_z, carry,
-                 mixed, mixed_x, weight, normed, resid, rows_in, hidden, narrow, part, part_x,
+                 mixed, mixed_x, weight, normed, resid, rows_in, hidden, narrow, part, part_x, kept,
                  load_sem, own_sem, table_send, table_recv, state_send, state_recv,
                  piece_send, piece_recv, mix_send, mix_recv, wo_send, wo_recv, part_send, part_recv,
                  row_sem, wide_sem, narrow_sem, done_sem):
@@ -491,13 +485,11 @@
     loads = []
     for h in range(heads):
         group = []
-        for n, (src, dst, width) in enumerate(((decay, cums, dk), (keys, k, dk), (queries, q, dk),
+        for n, (src, dst, width) in enumerate(((logits_w, logits, dk), (keys, k, dk), (queries, q, dk),
                                                (values, v, dv), (out_gate, og, dv))):
             group.append(pltpu.make_async_copy(src.at[:, h * width : (h + 1) * width], dst.at[h],
                                                load_sem.at[n, h]))
         loads.append(group)
-    doc_load = pltpu.make_async_copy(doc_wide, doc, load_sem.at[5, 0])
-    doc_load.start()
     for n in range(4):
         for h in range(heads):
             loads[h][n].start()
@@ -524,9 +516,21 @@
         mine = own.at[low:high] if len(full.shape) == 3 else own.at[:, low:high]
         ps.append(Piece(net, sends, mine, functools.partial(place, full, low, high),
                         piece_recv.at[i], piece_send.at[i], crossed))
-    gate_a_columns = pieces[0][2]
-    gate_a, up_a, gate_b, up_b, down_a, down_b, cross_a, cross_b = ps
-    gate_a.start()
+    downs = [p for p, (name, _, _, _) in zip(ps, pieces) if name == "d"]
+    gaps = iter(plan)
+
+    def tasks():
+        for kind, i, a in next(gaps):
+            if kind == 0:
+                ps[i].start_y()
+            elif kind == 1:
+                ps[i].start_z()
+            elif kind == 2:
+                ps[i].line(a)
+            else:
+                ps[i].beside(a)
+
+    tasks()
     mine_low = pl.multiple_of(t * half, half)
     away_low = pl.multiple_of((1 - t) * half, half)
     sends.go(out_weight.at[pl.ds(pl.multiple_of(c * quarter, quarter), quarter)],
@@ -538,16 +542,16 @@
         own_copies.append(pltpu.make_async_copy(
             own, place(full, 0, own.shape[len(full.shape) == 2], me), own_sem.at[i + 1]))
 
+    document_columns(blocks, size, doc_line, doc, doc_row)
     for h in range(heads):
         loads[h][0].wait()
-    doc_load.wait()
     table[0] = jnp.where(
         lax.broadcasted_iota(jnp.int32, table.shape[1:], 0) == FIRST,
         jnp.broadcast_to(doc[0:1, :], table.shape[1:]),
         jnp.broadcast_to(doc[rows - 1 : rows, :], table.shape[1:]))
 
     def sums(h, _):
-        prefix_sums(blocks, size, h, cums, table)
+        prefix_sums(blocks, size, h, logits, bias, extra, cums, table)
         return 0
 
     lax.fori_loop(0, heads, sums, 0)
@@ -559,10 +563,8 @@
         own_states(blocks, size, h, q, k, v, cums, doc, table, onward, rearward, tail, lead, states)
         return 0
 
-    lax.fori_loop(0, 1, state_of, 0)
-    for r in range(1, 4 * planes):
-        sends.go(table.at[0], table.at[r], table_send.at[r], table_recv.at[r], net.dev(r))
-    lax.fori_loop(1, heads, state_of, 0)
+    lax.fori_loop(0, heads, state_of, 0)
+    sends.go(table.at[0], table.at[1], table_send.at[0], table_recv.at[0], net.dev(SS))
     sends.go(states.at[c], from_sib, state_send.at[0], state_recv.at[0], net.dev(SS))
     for copy in own_copies:
         copy.start()
@@ -584,23 +586,27 @@
     def plane_log(a):
         return chip_log(a * 4) + chip_log(a * 4 + 2)
 
-    arrived(table.at[1], table_recv.at[1])
+    arrived(table.at[1], table_recv.at[0])
+    sends.go(table.at[0:2], table.at[2:4], table_send.at[1], table_recv.at[1], net.dev(YY))
     arrived(from_sib, state_recv.at[0])
     fade = jnp.where(leaves(1) == leaves(0), jnp.exp(state(0)), 0.0)
     way = 1 - c
     for h in range(heads):
         chip_state[h] = (states[way, h].astype(jnp.float32)
                          + column(fade, h) * from_sib[h].astype(jnp.float32)).astype(jnp.bfloat16)
+    tasks()
     sends.go(chip_state, from_y, state_send.at[1], state_recv.at[1], net.dev(YY))
 
     def inner_of(h, _):
         inner_outputs(blocks, size, h, q, k, v, cums, doc, doc_row, back, inner)
         return 0
 
+    tasks()
     lax.fori_loop(0, 2, inner_of, 0)
-    for r in range(2, 4 * planes):
-        arrived(table.at[r], table_recv.at[r])
+    tasks()
+    arrived(table.at[2:4], table_recv.at[1])
     arrived(from_y, state_recv.at[1])
+    tasks()
     upper = y == c
     fade = jnp.where(leaves(2) == leaves(0),
                      jnp.exp(jnp.where(upper, chip_log(0), chip_log(2))), 0.0)
@@ -610,20 +616,22 @@
         high = jnp.where(upper, mine, other)
         low = jnp.where(upper, other, mine)
         plane_state[h] = (high + column(fade, h) * low).astype(jnp.bfloat16)
+    tasks()
     early, late = [None], [None]
     for a in range(1, planes):
         below = net.zs[a] < z
         early.append((rising & below) | ((c == 0) & (net.zs[a] > z)))
         late.append((rising & (net.zs[a] > z)) | ((c == 0) & below))
     for a in range(1, planes):
+        sends.go(table.at[0:4], table.at[a * 4 : a * 4 + 4], table_send.at[1 + a],
+                 table_recv.at[1 + a], net.dev(a * 4), late[a])
         sends.go(plane_state, from_z.at[a - 1], state_send.at[1 + a], state_recv.at[1 + a],
                  net.dev(a * 4), late[a])
-    up_a.start_y()
-    up_a.start_s()
+    tasks()
     lax.fori_loop(2, heads, inner_of, 0)
-    up_a.start_z()
-    gate_a.near()
+    tasks()
     for a in range(1, planes):
+        arrived(table.at[a * 4 : a * 4 + 4], table_recv.at[1 + a], early[a])
         arrived(from_z.at[a - 1], state_recv.at[1 + a], early[a])
     entry = enters(1)
     fades = []
@@ -650,22 +658,22 @@
     sends.go(chip_carry, carry.at[way], state_send.at[5], state_recv.at[5], net.dev(SS))
     own_part = weight.at[pl.ds(pl.multiple_of((1 - t) * half + c * quarter, quarter), quarter)]
     sib_part = weight.at[pl.ds(pl.multiple_of((1 - t) * half + (1 - c) * quarter, quarter), quarter)]
-    arrived(own_part, wo_recv.at[0])
-    sends.go(own_part, own_part, wo_send.at[1], wo_recv.at[1], net.dev(SS))
-    weight_sent = sends.settle()
     for h in range(heads):
         loads[h][4].wait()
     arrived(carry.at[c], state_recv.at[5])
+    tasks()
+
+    def mix_send_of(h):
+        sends.go(mixed.at[h], mixed_x.at[h], mix_send.at[h], mix_recv.at[h], net.across())
+
     for h in range(heads):
         finished_head(h, 256, onward, rearward, inner, carry, og, head_gain, mixed)
+        tasks()
         if h:
-            sends.go(mixed.at[h - 1], mixed_x.at[h - 1], mix_send.at[h - 1], mix_recv.at[h - 1],
-                     net.across())
+            mix_send_of(h - 1)
+        tasks()
     own_copies[0].wait()
-    sends.go(mixed.at[heads - 1], mixed_x.at[heads - 1], mix_send.at[heads - 1],
-             mix_recv.at[heads - 1], net.across())
-    gate_a.far()
-    gate_b.start()
+    mix_send_of(heads - 1)
 
     step = rows_in.shape[1]
     steps = rows // step
@@ -685,19 +693,14 @@
 
     row_load(0, 0).start()
     lax.fori_loop(0, steps, own_product, 0)
-    up_a.near()
-    cross_a.start()
-    up_a.far()
-    gate_a.hand_over()
-    up_b.start()
-    gate_b.near()
-    cross_a.beside(0)
-    up_a.hand_over()
-    gate_b.far()
-    cross_b.start()
+    tasks()
+    arrived(own_part, wo_recv.at[0])
+    sends.go(own_part, own_part, wo_send.at[1], wo_recv.at[1], net.dev(SS))
+    weight_sent = sends.settle()
     for h in range(heads):
         arrived(mixed_x.at[h], mix_recv.at[h])
     arrived(sib_part, wo_recv.at[1])
+    tasks()
 
     def attend(i, _):
         slot = i % 2
@@ -725,16 +728,11 @@
         return 0
 
     lax.fori_loop(0, steps, attend, 0)
-    cross_a.near()
-    up_b.near()
-    cross_b.beside(0)
-    down_a.start()
+    tasks()
     own_copies[1].wait()
     own_copies[2].wait()
-    gate_a.siblings()
-    up_a.siblings()
-
-    columns = hidden.shape[1] // WIDE
+    weight_sent()
+
 
     def wide_at(slot, n):
         return pl.ds(pl.multiple_of((slot * 2 + n) * WIDE, WIDE), WIDE)
@@ -772,55 +770,39 @@
             copy.start()
         lax.fori_loop(begin, end, functools.partial(hidden_block, end), 0)
 
-    weight_sent()
-    cut = gate_a_columns // WIDE
-    hidden_blocks(0, cut)
-    up_b.far()
-    cross_a.far()
-    down_b.start()
-    gate_b.hand_over()
-    up_b.hand_over()
-    cross_b.near()
-    down_a.near()
-    gate_b.siblings()
-    up_b.siblings()
-    hidden_blocks(cut, columns)
-    down_b.near()
-    cross_b.far()
+    for needs, begin, end in groups:
+        for i in needs:
+            ps[i].siblings()
+        hidden_blocks(begin, end)
+        tasks()
     own_copies[3].wait()
-    downs = (down_a, down_b, cross_a, cross_b)
 
     order = [(a, b) for a in range(planes) for b in range(2)]
     lanes = narrow.shape[2] // 2
     here = pl.ds(pl.multiple_of(t * share, share), share)
     there = pl.ds(pl.multiple_of((1 - t) * share, share), share)
-
-    def narrow_load(n):
-        pair = net.chip(order[n][0] * 4 + order[n][1] * 2) * 2
-        return [pltpu.make_async_copy(down_full.at[pair + m],
-                                      narrow.at[n % 2, :, m * lanes : (m + 1) * lanes],
-                                      narrow_sem.at[n % 2, m]) for m in range(2)]
-
-    for a in range(planes):
-        if a == 3:
-            down_a.far()
-            down_b.far()
-        down_a.beside(a)
-        down_b.beside(a)
-        for b in range(2):
-            for p in downs:
-                p.sibling(a, b)
-            for copy in narrow_load(a * 2 + b):
-                copy.start()
-        for b in range(2):
-            n = a * 2 + b
-            for copy in narrow_load(n):
-                copy.wait()
-            part[n] = product(hidden[there, :], narrow[b]).astype(jnp.bfloat16)
-            kept = product(hidden[here, :], narrow[b]).astype(jnp.bfloat16)
-            sends.go(part.at[n], part_x.at[n], part_send.at[n], part_recv.at[n], net.across())
-            block = net.chip(a * 4 + b * 2)
-            resid[block] = resid[block] + kept.astype(jnp.float32)
+    for n, (a, b) in enumerate(order):
+        for p in downs:
+            p.sibling(a, b)
+        block = net.chip(a * 4 + b * 2)
+        last_block = net.chip(order[n - 1][0] * 4 + order[n - 1][1] * 2)
+        copies = [pltpu.make_async_copy(down_full.at[block * 2 + m],
+                                        narrow.at[b, :, m * lanes : (m + 1) * lanes],
+                                        narrow_sem.at[b, m]) for m in range(2)]
+        for copy in copies:
+            copy.start()
+        if n:
+            kept[...] = product(hidden[here, :], narrow[1 - b]).astype(jnp.bfloat16)
+        for copy in copies:
+            copy.wait()
+        part[n] = product(hidden[there, :], narrow[b]).astype(jnp.bfloat16)
+        if n:
+            resid[last_block] = resid[last_block] + kept[...].astype(jnp.float32)
+        sends.go(part.at[n], part_x.at[n], part_send.at[n], part_recv.at[n], net.across())
+        tasks()
+    block = net.chip(order[-1][0] * 4 + order[-1][1] * 2)
+    away = product(hidden[here, :], narrow[order[-1][1]]).astype(jnp.bfloat16)
+    resid[block] = resid[block] + away.astype(jnp.float32)
     outs = []
     for n in range(len(order)):
         block = net.chip(order[n][0] * 4 + order[n][1] * 2)
@@ -835,11 +817,64 @@
     sends.drain()
 
 
+PLAN = (
+    ((1, 0, 0), (0, 0, 0),),
+    (),
+    (),
+    (),
+    ((0, 1, 0),),
+    (),
+    ((2, 0, 1), (1, 1, 0), (2, 0, 2),),
+    ((0, 5, 0), (0, 6, 0), (2, 0, 3),),
+    (),
+    ((3, 1, 0), (0, 3, 0),),
+    ((1, 2, 0),),
+    (),
+    ((0, 2, 0),),
+    (),
+    ((1, 3, 0),),
+    (),
+    ((2, 1, 1),),
+    ((1, 5, 0), (3, 0, 1), (3, 0, 3), (3, 0, 2), (3, 0, 0), (2, 1, 2), (2, 2, 1), (3, 3, 0), (2, 1, 3), (3, 1, 1), (2, 2, 2),),
+    ((2, 2, 3),),
+    ((3, 1, 2), (2, 3, 1), (3, 1, 3), (2, 3, 2), (1, 4, 0),),
+    (),
+    ((3, 5, 0), (3, 2, 0), (2, 3, 3), (2, 5, 1),),
+    ((3, 3, 3), (0, 4, 0), (1, 6, 0), (3, 6, 0), (3, 2, 1), (3, 2, 3), (3, 3, 1), (3, 3, 2), (2, 5, 2), (3, 2, 2),),
+    ((3, 5, 1),),
+    (),
+    ((3, 4, 0),),
+    ((2, 4, 1),),
+    ((2, 4, 2), (2, 5, 3), (2, 6, 1),),
+    ((3, 4, 1), (2, 6, 2), (3, 5, 2), (3, 4, 2), (3, 6, 1),),
+    (),
+    ((2, 4, 3), (3, 6, 2), (2, 6, 3), (3, 4, 3),),
+    (),
+    ((3, 6, 3), (3, 5, 3),),
+    (),
+)
+
+
 def pieces_of(units):
-    half = (units // WIDE + 1) // 2 * WIDE
-    pieces = [(w, a, b, False) for a, b in ((0, half), (half, units)) for w in "gu"]
-    return pieces + [("d", units * i // 4, units * (i + 1) // 4, i >= 2) for i in range(4)]
-
+    block = units // 11
+    pieces = [
+        ("g", block * 0, block * 6, False),
+        ("u", block * 0, block * 6, False),
+        ("g", block * 6, block * 11, False),
+        ("u", block * 6, block * 11, False),
+        ("d", units * 0 // 176, units * 66 // 176, False),
+        ("d", units * 66 // 176, units * 132 // 176, False),
+        ("d", units * 132 // 176, units * 176 // 176, True),
+    ]
+    groups = (
+        ((0, 1), 0, 2),
+        ((), 2, 4),
+        ((), 4, 6),
+        ((2, 3), 6, 8),
+        ((), 8, 10),
+        ((), 10, 11),
+    )
+    return pieces, groups
 
 def whole_layer(stream, queries, projected_keys, values, decay_gate_logits, decay_gate_bias,
                 extra_log_decay, document_index, output_gate, head_norm_gain, output_weight,
@@ -855,12 +890,7 @@
     share = rows // 2
     units = gate_weight.shape[1]
     chips = devices // 2
-    decay = jax.nn.log_sigmoid(decay_gate_logits.astype(jnp.float32) + decay_gate_bias) / TAU
-    decay = (decay.reshape(rows, heads, dk) + extra_log_decay[:, :, None]).reshape(rows, -1)
-    doc = document_index.astype(jnp.float32)
-    doc_wide = jnp.broadcast_to(doc[:, None], (rows, dk))
-    doc_row = doc.reshape(blocks, size)
-    pieces = pieces_of(units)
+    pieces, groups = pieces_of(units)
     any_, vm = pl.BlockSpec(memory_space=pl.ANY), pl.BlockSpec(memory_space=pltpu.VMEM)
     b16, f32 = jnp.bfloat16, jnp.float32
     dma = pltpu.SemaphoreType.DMA
@@ -868,8 +898,9 @@
     step = 256
     scratch = [
         pltpu.VMEM((heads, rows, dk), b16), pltpu.VMEM((heads, rows, dk), b16),
-        pltpu.VMEM((heads, rows, dv), b16), pltpu.VMEM((heads, rows, dk), f32),
-        pltpu.VMEM((rows, dk), f32), pltpu.VMEM((heads, rows, dv), b16),
+        pltpu.VMEM((heads, rows, dv), b16), pltpu.VMEM((heads, rows, dk), b16),
+        pltpu.VMEM((heads, rows, dk), f32), pltpu.VMEM((rows, dk), f32),
+        pltpu.VMEM((blocks, size), f32), pltpu.VMEM((heads, rows, dv), b16),
         pltpu.VMEM((heads, rows, dk), b16), pltpu.VMEM((heads, rows, dk), b16),
         pltpu.VMEM((heads, rows, dv), f32), pltpu.VMEM((rows, dk), b16), pltpu.VMEM((rows, dk), b16),
         pltpu.VMEM((blocks, dk, dv), b16),
@@ -882,25 +913,26 @@
         pltpu.VMEM((chips, share, WIDE), f32), pltpu.VMEM((2, step, width), b16),
         pltpu.VMEM((rows, units), b16),
         pltpu.VMEM((2, units, WIDE), b16), pltpu.VMEM((chips, share, WIDE), b16),
-        pltpu.VMEM((chips, share, WIDE), b16),
-        dma((6, heads)), dma((4,)), dma((devices,)), dma((devices,)), dma((8,)), dma((8,)),
+        pltpu.VMEM((chips, share, WIDE), b16), pltpu.VMEM((share, WIDE), b16),
+        dma((6, heads)), dma((4,)), dma((8,)), dma((8,)), dma((8,)), dma((8,)),
         dma((len(pieces), 24)), dma((len(pieces), devices)), dma((heads,)), dma((heads,)),
         dma((2,)), dma((2,)), dma((chips,)), dma((chips,)), dma((2,)), dma((2, 2)), dma((2, 2)),
         dma((chips,)),
     ]
     result = pl.pallas_call(
-        functools.partial(layer_kernel, planes, size, pieces),
+        functools.partial(layer_kernel, planes, size, pieces, PLAN, groups),
         out_shape=[
             jax.ShapeDtypeStruct(shape, b16)
             for shape in ((share, width), (devices * gate_weight.shape[0], units),
                           (devices * up_weight.shape[0], units), (devices,) + down_weight.shape)],
-        in_specs=[any_] * 6 + [vm, any_, vm, any_, vm, any_, any_, any_],
+        in_specs=[any_] * 5 + [vm, vm, vm, any_, vm, any_, vm, any_, any_, any_],
         out_specs=[any_] * 4,
         scratch_shapes=scratch,
         compiler_params=pltpu.CompilerParams(collective_id=0, has_side_effects=True,
                                              vmem_limit_bytes=67043328),
         name="whole_layer",
-    )(stream, queries, projected_keys, values, decay, doc_wide, doc_row, output_gate,
+    )(stream, queries, projected_keys, values, decay_gate_logits,
+      decay_gate_bias.reshape(heads, dk), extra_log_decay.T, document_index[None], output_gate,
       head_norm_gain.astype(f32)[None], output_weight, feedforward_norm_gain.astype(f32)[None],
       gate_weight, up_weight, down_weight)
     return result[0]

time: 265 us -> 238 us (0.90)
  Pallas kernels: 251 us -> 232 us
  local copies, waits for them, and re-layouts: 6.98 us -> 3.16 us
  other arithmetic: 6.03 us -> 2.45 us
    pallas_call x1, Pallas kernels: 251 us -> 232 us  [whole_layer(): pl.pallas_call(functools.partial(layer_kernel, planes, size, pieces, PLAN...]
    add x1 -> x0, other arithmetic: 2.75 us -> none  [whole_layer(): decay.reshape(rows, heads, dk) + extra_log_decay[:, :, None]]
where the time goes in v2:
time: 238 us
  Pallas kernels  232 us (97%)
  local copies, waits for them, and re-layouts  3.16 us (1%)
  other arithmetic  2.45 us (1%)
    pallas_call x1, Pallas kernels, whole_layer(): pl.pallas_call(functools.partial(layer_kernel, planes, size, pieces, PLAN...  232 us

profile of v2, /device:TPU:0, one launch (start us, length us, event | category | flops | bytes accessed | tf_op | source)
XLA Modules:
  0.0 237.7 jit_solution(16868719960509631775)
XLA Ops:
  0.0 1.2 broadcast_in_dim.18
  1.2 1.3 broadcast_in_dim.19
  2.5 232.1 %whole_layer.1 = (bf16[512,2048]{1,0:T(8,128)(2,1)}, bf16[2048,2816]{1,0:T(8,128)(2,1)}, bf16[2048,2816]{1,0:T(8,128)(2,1)}, bf16[16,2816,128]{2,1,0:T(8,128)(2,1)}) custom-call(bf16[1024,2048]{1,0:T(8,128)(2,1)} %stream.1, bf16[1024,512]{1,0:T(8,128)(2,1)} %queries.1, bf16[1024,512]{1,0:T(8,128)(2,1)} %keys.1, bf16[1024,1024]{1,0:T(8,128)(2,1)} %values.1, ...), custom_call_target="tpu_custom_call" | custom-call | tf_op jit(solution)/shard_map/whole_layer/pallas_call | solution.py:922
  234.5 3.2 %copy.17 = bf16[512,2048]{1,0:T(8,128)(2,1)} copy(bf16[512,2048]{1,0:T(8,128)(2,1)} %get-tuple-element.6) | data formatting | bytes 4194304
